TPU v7x, 512 devices: a whole 4x4x16 slice. The times are simulated.
512 devices in a mesh: kv: 64 (over z, y), tp: 8 (over x, core).
Axes of the slice: x: 4, y: 4, z: 16, core: 2. Of those that a mesh axis runs over, the one named last changes fastest.
Arguments:
- tokens: bfloat16 [16384, 2048], P('kv'), may hold values from -72 to 72
- w_query: bfloat16 [2048, 1024], P(None, 'tp'), may hold values from -0.125 to 0.125
- w_key: bfloat16 [2048, 1024], P(None, 'tp'), may hold values from -0.125 to 0.125
- w_value: bfloat16 [2048, 1024], P(None, 'tp'), may hold values from -0.125 to 0.125
- w_out: bfloat16 [1024, 2048], P('tp'), may hold values from -0.1875 to 0.1875
- chosen: int32 [256, 16], replicated, may hold values from -1 to 255, as said below
Outputs:
- mixed: bfloat16 [16384, 2048], P(('kv', 'tp'))
- log_sums: float32 [16, 16384], P('tp', 'kv')
Inputs may be any that keep to these rules, and one draw needn't show every extreme that they name: `chosen`: row b begins with b itself, then lists distinct key blocks at most b, then holds -1 in its remaining entries. Taken together, the rows of the query blocks of one index of kv list at most 2 distinct blocks of the positions of any other index of kv, and exactly 2 for some pairs of indices in every draw.
All inputs are finite; a program needn't handle non-finite values.
Results may differ from a plain program's by a relative error of at most 0.03.
Values may be sent and summed in bfloat16 or wider, within the bound.
A program may use at most 64 MiB of HBM per device.

v0:
```python
import jax
import jax.numpy as jnp
from jax import lax
from jax.sharding import PartitionSpec as P

HEAD_DIM = 64
BLK = 64
SEL = 16
CAP = 2


rotary_base = 500000.0
masked_score = -1e30


def in_blocks(value, dim, size):
    before, after = (value.shape[:dim], value.shape[dim + 1 :])
    return jnp.moveaxis(value.reshape(*before, size, -1, *after), dim, 0)


def summed_on_arrival(value, axis, dim):
    size = lax.axis_size(axis)
    tiles = lax.all_to_all(in_blocks(value, dim, size), axis, 0, 0, tiled=True)
    return jnp.sum(tiles.astype(jnp.float32), axis=0)


def rotate(values, positions, head_count, head_size):
    half_size = head_size // 2
    inverse = rotary_base ** (-jnp.arange(half_size, dtype=jnp.float32) / half_size)
    angles = positions.astype(jnp.float32)[:, None, None] * inverse[None, None, :]
    cos_part = jnp.cos(angles)
    sin_part = jnp.sin(angles)
    grouped = values.reshape(values.shape[0], head_count, head_size)
    first_half = grouped[..., :half_size]
    second_half = grouped[..., half_size:]
    turned = jnp.concatenate(
        [
            first_half * cos_part - second_half * sin_part,
            second_half * cos_part + first_half * sin_part,
        ],
        axis=-1,
    )
    return turned.reshape(values.shape)


def local(tokens, w_query, w_key, w_value, w_out, chosen):
    local_rows = tokens.shape[0]
    local_width = w_query.shape[1]
    head_count = local_width // HEAD_DIM
    scaling = HEAD_DIM ** (-0.5)
    device = lax.axis_index("kv")
    positions = device * local_rows + jnp.arange(local_rows)
    query = rotate(
        jnp.dot(tokens, w_query, preferred_element_type=jnp.float32),
        positions,
        head_count,
        HEAD_DIM,
    ).astype(jnp.bfloat16)
    keys_here = rotate(
        jnp.dot(tokens, w_key, preferred_element_type=jnp.float32), positions, head_count, HEAD_DIM
    ).astype(jnp.bfloat16)
    values_here = jnp.dot(tokens, w_value, preferred_element_type=jnp.float32).astype(jnp.bfloat16)
    blocks_here = local_rows // BLK
    own_lists = lax.dynamic_slice_in_dim(chosen, device * blocks_here, blocks_here, 0)
    query_heads = query.reshape(local_rows, head_count, HEAD_DIM)
    devices = lax.axis_size("kv")
    mine_blocks = device * blocks_here + jnp.arange(blocks_here)
    listed_hits = jnp.any(chosen[:, :, None] == mine_blocks[None, None, :], axis=1)
    wanted = jnp.any(listed_hits.reshape(devices, blocks_here, blocks_here), axis=1)
    wanted = wanted & (jnp.arange(devices) != device)[:, None]
    send_slots = jnp.cumsum(wanted.astype(jnp.int32), axis=1) - 1
    placing = (wanted[:, None, :] & (send_slots[:, None, :] == jnp.arange(CAP)[:, None])).astype(
        jnp.bfloat16
    )
    both_here = jnp.concatenate([keys_here, values_here], axis=1).reshape(
        blocks_here, BLK, 2 * local_width
    )
    outgoing = (
        jnp.einsum("dcb,bkf->dckf", placing, both_here, preferred_element_type=jnp.float32)
        .astype(jnp.bfloat16)
        .reshape(devices, CAP * BLK, 2 * local_width)
    )
    incoming = lax.all_to_all(outgoing, "kv", split_axis=0, concat_axis=0, tiled=True)
    every_block = jnp.arange(chosen.shape[0])
    needed = jnp.any(own_lists.reshape(-1)[:, None] == every_block[None, :], axis=0).reshape(
        devices, blocks_here
    )
    my_slots = (jnp.cumsum(needed.astype(jnp.int32), axis=1) - 1).reshape(-1)
    usable = own_lists >= 0
    safe_rows = jnp.maximum(own_lists, 0)
    lookup = jnp.sum(
        jnp.where(safe_rows[:, :, None] == every_block[None, None, :], my_slots[None, None, :], 0),
        axis=-1,
    )
    owner_dev = safe_rows // blocks_here
    source_row = jnp.where(
        owner_dev == device, devices * CAP + safe_rows % blocks_here, owner_dev * CAP + lookup
    )
    key_table = jnp.concatenate(
        [incoming.reshape(devices * CAP, BLK, 2 * local_width), both_here], axis=0
    )
    picked = key_table[source_row]
    picked_keys = picked[..., :local_width].reshape(blocks_here, SEL * BLK, head_count, HEAD_DIM)
    picked_values = picked[..., local_width:].reshape(blocks_here, SEL * BLK, head_count, HEAD_DIM)
    query_blocks = query_heads.reshape(blocks_here, BLK, head_count, HEAD_DIM)
    scores = (
        jnp.einsum("bqhd,bkhd->bhqk", query_blocks, picked_keys, preferred_element_type=jnp.float32)
        * scaling
    )
    key_mask = jnp.broadcast_to(usable[:, :, None], (blocks_here, SEL, BLK)).reshape(
        blocks_here, 1, 1, SEL * BLK
    )
    scores = jnp.where(key_mask, scores, masked_score)
    block_max = jnp.max(scores, axis=-1)
    weights = jnp.where(key_mask, jnp.exp(scores - block_max[..., None]), 0.0)
    block_total = jnp.sum(weights, axis=-1)
    block_sum = jnp.einsum(
        "bhqk,bkhd->bhqd",
        weights.astype(jnp.bfloat16),
        picked_values,
        preferred_element_type=jnp.float32,
    )
    row_max = jnp.transpose(block_max, (1, 0, 2)).reshape(head_count, local_rows)
    totals = jnp.transpose(block_total, (1, 0, 2)).reshape(head_count, local_rows)
    summed = jnp.transpose(block_sum, (1, 0, 2, 3)).reshape(head_count, local_rows, HEAD_DIM)
    mixed_heads = summed / totals[..., None]
    attended = (
        jnp.transpose(mixed_heads, (1, 0, 2)).reshape(local_rows, local_width).astype(jnp.bfloat16)
    )
    log_sums = row_max + jnp.log(totals)
    output = summed_on_arrival(
        jnp.dot(attended, w_out, preferred_element_type=jnp.float32).astype(jnp.bfloat16), "tp", 0
    )
    return (output.astype(jnp.bfloat16), log_sums)


def solution(mesh):
    placed = (P("kv", None), P(None, "tp"), P(None, "tp"), P(None, "tp"), P("tp", None), P())
    return jax.shard_map(
        local,
        mesh=mesh,
        in_specs=placed,
        out_specs=(P(("kv", "tp"), None), P("tp", "kv")),
        check_vma=False,
    )
```

profile of v0, /device:TPU:1, one launch (start us, length us, event | category | flops | bytes accessed | tf_op | source)
XLA Modules:
  0.0 270.5 jit_solution(12492361866420358039)
XLA Ops:
  0.6 0.0 copy-start
  0.6 0.0 copy-start.1
  0.7 1.2 copy-done
  1.9 1.5 fusion.33
  3.4 0.0 copy-start.2
  3.4 1.5 fusion.34
  4.9 0.0 copy-done.1
  5.0 0.5 convolution_convert_fusion.2
  5.4 0.2 multiply_cosine_fusion
  5.7 0.1 copy.77
  5.8 0.0 copy-done.2
  5.9 0.1 compare_reduce_fusion
  5.9 0.2 reshape.174
  6.1 0.1 reduce_or.28
  6.3 1.3 convolution_convert_fusion
  7.6 4.3 %copy.79 = bf16[64,128,256]{2,1,0:T(8,128)(2,1)} copy(bf16[64,128,256]{2,0,1:T(8,128)(2,1)S(1)} %bitcast.41) | data formatting | bytes 8388608 | tf_op jit(solution)/shard_map/reshape | solution.py:81
  12.0 19.7 %all-to-all-start = ((bf16[64,128,256]{2,1,0:T(8,128)(2,1)}), bf16[64,128,256]{2,1,0:T(8,128)(2,1)}, u32[]{:S(2)}, u32[]{:S(2)}) async-start(bf16[64,128,256]{2,1,0:T(8,128)(2,1)} %copy.79), calls=%async_computation | async-start | bytes 8388608 | tf_op jit(solution)/shard_map/all_to_all | solution.py:83
  31.7 0.1 constant_dynamic-slice_fusion
  31.8 0.1 copy.92
  31.9 0.1 eq.73
  32.0 0.1 fusion.19
  32.1 0.1 reshape.184
  32.2 0.1 copy.80
  32.3 0.1 copy.81
  32.4 0.1 sub.33
  32.5 0.2 select_reduce_fusion
  32.8 0.1 reshape.187
  32.8 0.1 convert_element_type.55
  33.0 0.1 broadcast_in_dim.54
  33.1 0.1 broadcast_in_dim.55
  33.2 182.2 %all-to-all-done = bf16[64,128,256]{2,1,0:T(8,128)(2,1)} async-done(((bf16[64,128,256]{2,1,0:T(8,128)(2,1)}), bf16[64,128,256]{2,1,0:T(8,128)(2,1)}, u32[]{:S(2)}, u32[]{:S(2)}) %all-to-all-start) | async-done | bytes 4194336 | tf_op jit(solution)/shard_map/all_to_all | solution.py:83
  215.4 4.5 %pad_maximum_fusion = bf16[132,64,256]{2,1,0:T(8,128)(2,1)} fusion(bf16[4,64,256]{2,1,0:T(8,128)(2,1)S(1)} %bitcast.44, bf16[128,64,256]{2,1,0:T(8,128)(2,1)} %bitcast.8), kind=kLoop, calls=%fused_computation.1 | loop fusion | flops 2162688 | bytes 8650752 | tf_op jit(solution)/shard_map/concatenate | solution.py:99
  219.9 2.9 %gather_fusion = bf16[64,64,256]{2,1,0:T(8,128)(2,1)S(1)} fusion(bf16[132,64,256]{2,1,0:T(8,128)(2,1)} %pad_maximum_fusion, s32[1024]{0:T(1024)S(1)} %pad_clamp_fusion), kind=kCustom, calls=%fused_computation | custom fusion | bytes 4194560 | tf_op jit(solution)/shard_map/gather | solution.py:102
  222.8 1.9 fusion.32
  224.7 5.0 %reshape.197 = bf16[4,1024,2,64]{3,2,1,0:T(2,128)(2,1)} reshape(bf16[4,16,64,128]{3,2,1,0:T(8,128)(2,1)} %get-tuple-element.4) | data formatting | bytes 2097152 | tf_op jit(solution)/shard_map/reshape | solution.py:103
  229.8 2.6 fusion.4
  232.3 0.7 fusion.5
  233.0 0.1 div.25
  233.1 5.0 %reshape.198 = bf16[4,1024,2,64]{3,2,1,0:T(2,128)(2,1)} reshape(bf16[4,16,64,128]{3,2,1,0:T(8,128)(2,1)} %get-tuple-element.5) | data formatting | bytes 2097152 | tf_op jit(solution)/shard_map/reshape | solution.py:104
  238.1 2.4 fusion.7
  240.5 0.1 copy.85
  240.6 0.2 reshape.181
  240.9 2.5 convolution_convert_fusion.1
  243.4 11.4 %all-to-all-start.1 = ((bf16[8,32,2048]{2,1,0:T(8,128)(2,1)}), bf16[8,32,2048]{2,1,0:T(8,128)(2,1)S(1)}, u32[]{:S(2)}, u32[]{:S(2)}) async-start(bf16[8,32,2048]{2,1,0:T(8,128)(2,1)} %bitcast.14), calls=%async_computation.1 | async-start | bytes 2097152 | tf_op jit(solution)/shard_map/all_to_all | solution.py:23
  254.7 0.1 reshape.183
  254.8 0.6 log_add_fusion
  255.4 14.3 %all-to-all-done.1 = bf16[8,32,2048]{2,1,0:T(8,128)(2,1)S(1)} async-done(((bf16[8,32,2048]{2,1,0:T(8,128)(2,1)}), bf16[8,32,2048]{2,1,0:T(8,128)(2,1)S(1)}, u32[]{:S(2)}, u32[]{:S(2)}) %all-to-all-start.1) | async-done | bytes 1048608 | tf_op jit(solution)/shard_map/all_to_all | solution.py:23
  269.7 0.8 reduce_sum.32
  (20 shorter events, 0.2 us)
Async XLA Ops:
  0.6 1.2 copy-start
  0.6 4.3 %copy-start.1 = (bf16[2048,128]{1,0:T(8,128)(2,1)S(1)}, bf16[2048,128]{1,0:T(8,128)(2,1)}, u32[]{:S(2)}) copy-start(bf16[2048,128]{1,0:T(8,128)(2,1)} %param.9) | copy-start | bytes 1572868
  3.4 2.5 copy-start.2
  12.0 203.4 %all-to-all-start = ((bf16[64,128,256]{2,1,0:T(8,128)(2,1)}), bf16[64,128,256]{2,1,0:T(8,128)(2,1)}, u32[]{:S(2)}, u32[]{:S(2)}) async-start(bf16[64,128,256]{2,1,0:T(8,128)(2,1)} %copy.79), calls=%async_computation | async-start | bytes 8388608 | tf_op jit(solution)/shard_map/all_to_all | solution.py:83
  243.4 26.3 %all-to-all-start.1 = ((bf16[8,32,2048]{2,1,0:T(8,128)(2,1)}), bf16[8,32,2048]{2,1,0:T(8,128)(2,1)S(1)}, u32[]{:S(2)}, u32[]{:S(2)}) async-start(bf16[8,32,2048]{2,1,0:T(8,128)(2,1)} %bitcast.14), calls=%async_computation.1 | async-start | bytes 2097152 | tf_op jit(solution)/shard_map/all_to_all | solution.py:23
where the time goes:
time: 271 us; the launch traced here: 270 us
  waiting for transfers between devices  196 us (72%)
  starting transfers between devices  31.1 us (11%)
  local copies, waits for them, and re-layouts  22.2 us (8%)
  matrix products  12.3 us (5%)
  other arithmetic  7.6 us (3%)
    all_to_all x1, waiting for transfers between devices, local(): lax.all_to_all(outgoing, 'kv', split_axis=0, concat_axis=0, tiled=True)  182 us
    all_to_all x1, starting transfers between devices, local(): lax.all_to_all(outgoing, 'kv', split_axis=0, concat_axis=0, tiled=True)  19.7 us
    all_to_all x1, waiting for transfers between devices, summed_on_arrival(): tiles = lax.all_to_all(in_blocks(value, dim, size), axis, 0, 0, tiled=True)  14.3 us
    all_to_all x1, starting transfers between devices, summed_on_arrival(): tiles = lax.all_to_all(in_blocks(value, dim, size), axis, 0, 0, tiled=True)  11.4 us
  transfers between devices with their start and end apart: 2, of which 2 were waited for; matrix products, arithmetic and copies ran while one was open for 1% of the time, Pallas kernels for 0%

commit v1 on v0

v1 whole, which is shorter than its diff:
```python
import functools

import jax
import jax.numpy as jnp
from jax import lax
from jax.experimental import pallas as pl
from jax.experimental.pallas import tpu as pltpu
from jax.sharding import PartitionSpec as P

HEAD_DIM = 64
BLK = 64
SEL = 16
NY = 4
ROTARY_BASE = 500000.0
MASKED = -1e30
MESH = pl.DeviceIdType.MESH


def rotary_tables(positions, width):
    half = HEAD_DIM // 2
    lane = jnp.arange(width)
    inverse = ROTARY_BASE ** (-(lane % half).astype(jnp.float32) / half)
    angles = positions.astype(jnp.float32)[:, None] * inverse[None, :]
    sign = jnp.where(lane % HEAD_DIM < half, -1.0, 1.0)
    return jnp.cos(angles), jnp.sin(angles) * sign[None, :]


def turn(values, cos_part, sin_part):
    width = values.shape[1]
    half = HEAD_DIM // 2
    lane = lax.broadcasted_iota(jnp.int32, values.shape, 1)
    ahead = pltpu.roll(values, width - half, 1)
    behind = pltpu.roll(values, half, 1)
    partner = jnp.where(lane % HEAD_DIM < half, ahead, behind)
    return values * cos_part + partner * sin_part


def project(tokens_ref, wq_ref, wk_ref, wv_ref, cos_ref, sin_ref, kv_ref, q_ref):
    blocks = kv_ref.shape[0]
    width = wk_ref.shape[1]
    cos_part, sin_part = cos_ref[...], sin_ref[...]
    tokens = tokens_ref[...]
    keys = jnp.dot(tokens, wk_ref[...], preferred_element_type=jnp.float32)
    keys = turn(keys, cos_part, sin_part).astype(jnp.bfloat16)
    kv_ref[:, :, :width] = keys.reshape(blocks, BLK, width)
    values = jnp.dot(tokens, wv_ref[...], preferred_element_type=jnp.float32).astype(jnp.bfloat16)
    kv_ref[:, :, width:] = values.reshape(blocks, BLK, width)
    query = jnp.dot(tokens, wq_ref[...], preferred_element_type=jnp.float32)
    query = turn(query, cos_part, sin_part).astype(jnp.bfloat16).astype(jnp.float32)
    query = query * HEAD_DIM ** (-0.5)
    lane = lax.broadcasted_iota(jnp.int32, query.shape, 1)
    for head in range(width // HEAD_DIM):
        mine = jnp.where(lane // HEAD_DIM == head, query, 0.0).astype(jnp.bfloat16)
        q_ref[:, head * BLK : (head + 1) * BLK, :] = mine.reshape(blocks, BLK, width)


def attend(
    nz,
    ntp,
    kv_ref,
    q_ref,
    w_ref,
    bias_ref,
    sel_ref,
    idx_ref,
    out_ref,
    lse_ref,
    pool,
    to_right,
    to_left,
    picked,
    wall,
    att,
    abuf,
    up_send,
    up_recv,
    dn_send,
    dn_recv,
    rs_send,
    rs_recv,
    ls_send,
    ls_recv,
    rf_send,
    rf_recv,
    lf_send,
    lf_recv,
    w_send,
    w_recv,
    a_send,
    a_recv,
):
    kv = lax.axis_index("kv")
    tp = lax.axis_index("tp")
    z, y = kv // NY, kv % NY
    nx = ntp // 2
    x, core = tp // 2, tp % 2
    up = ((z + 1) % nz) * NY + y
    down = ((z + nz - 1) % nz) * NY + y
    right = z * NY + (y + 1) % NY
    left = z * NY + (y + NY - 1) % NY
    x_right = ((x + 1) % nx) * 2 + core
    x_left = ((x + nx - 1) % nx) * 2 + core
    partner = x * 2 + (1 - core)
    blocks = kv_ref.shape[0]
    width = w_ref.shape[0]
    left_base = nz * blocks
    right_base = left_base + 3 * nz
    far0_base = right_base + 3 * nz
    far1_base = far0_base + nz
    rows = att.shape[0] // ntp

    barrier = pltpu.get_barrier_semaphore()
    for peer in (up, down, right, left):
        pl.semaphore_signal(barrier, inc=1, device_id=(peer, tp), device_id_type=MESH)
    for step in range(1, ntp):
        pl.semaphore_signal(
            barrier, inc=1, device_id=(kv, (tp + step) % ntp), device_id_type=MESH
        )
    pl.semaphore_wait(barrier, 4 + ntp - 1)

    def remote(src, dst, send, recv, device):
        return pltpu.make_async_remote_copy(
            src_ref=src,
            dst_ref=dst,
            send_sem=send,
            recv_sem=recv,
            device_id=device,
            device_id_type=MESH,
        )

    ups = (nz - 1 + 1) // 2
    downs = nz - 1 - ups

    def plane(p):
        return pool.at[pl.ds(p * blocks, blocks)]

    def up_copy(step):
        p = (z + nz - step) % nz
        src = kv_ref if step == 0 else plane(p)
        return remote(src, plane(p), up_send.at[step], up_recv.at[step], (up, tp))

    def down_copy(step):
        p = (z + step) % nz
        src = kv_ref if step == 0 else plane(p)
        return remote(src, plane(p), dn_send.at[step], dn_recv.at[step], (down, tp))

    def right_copy(p):
        dst = pool.at[pl.ds(left_base + 3 * p, 3)]
        return remote(to_right.at[p], dst, rs_send.at[p], rs_recv.at[p], (right, tp))

    def left_copy(p):
        dst = pool.at[pl.ds(right_base + 3 * p, 3)]
        return remote(to_left.at[p], dst, ls_send.at[p], ls_recv.at[p], (left, tp))

    def right_relay(p):
        src = pool.at[left_base + 3 * p + 2]
        return remote(src, pool.at[far0_base + p], rf_send.at[p], rf_recv.at[p], (right, tp))

    def left_relay(p):
        src = pool.at[right_base + 3 * p + 2]
        return remote(src, pool.at[far1_base + p], lf_send.at[p], lf_recv.at[p], (left, tp))

    def exchange(p):
        here = [pool[p * blocks + b] for b in range(blocks)]

        def pick(ahead, c):
            which = sel_ref[(p * 3 + ahead - 1) * 2 + c]
            found = here[blocks - 1]
            for b in range(blocks - 1):
                found = jnp.where(which == b, here[b], found)
            return found

        to_right[p, 0] = pick(1, 0)
        to_right[p, 1] = pick(1, 1)
        to_right[p, 2] = pick(2, 0)
        right_copy(p).start()
        to_left[p, 0] = pick(3, 0)
        to_left[p, 1] = pick(3, 1)
        to_left[p, 2] = pick(2, 1)
        left_copy(p).start()

    def relay(p):
        right_copy(p).wait_recv()
        right_relay(p).start()
        left_copy(p).wait_recv()
        left_relay(p).start()

    def settle(p):
        right_relay(p).wait()
        left_relay(p).wait()
        right_copy(p).wait_send()
        left_copy(p).wait_send()

    half = width // 2

    def w_ring(side):
        src = w_ref
        peer = x_right if side == 0 else x_left
        return remote(src, wall.at[tp], w_send.at[side], w_recv.at[side], (kv, peer))

    def w_half(side):
        origin = x_left if side == 0 else x_right
        peer = x_right if side == 0 else x_left
        part = wall.at[origin, pl.ds(side * half, half)]
        return remote(part, part, w_send.at[2 + side], w_recv.at[2 + side], (kv, peer))

    def w_pair(which):
        far = ((x + 2) % nx) * 2 + core
        owner = (tp, x_left, x_right, far)[which]
        src = w_ref if which == 0 else wall.at[owner]
        return remote(src, wall.at[owner], w_send.at[4 + which], w_recv.at[4 + which], (kv, partner))

    up_copy(0).start()
    down_copy(0).start()
    w_ring(0).start()
    w_ring(1).start()
    w_pair(0).start()
    pool[pl.ds(z * blocks, blocks)] = kv_ref[...]
    wall[tp] = w_ref[...]
    exchange(z)

    order = [[(z, None)]]
    for step in range(ups):
        up_copy(step).wait_recv()
        if step + 1 < ups:
            up_copy(step + 1).start()
        if step < downs:
            down_copy(step).wait_recv()
            if step + 1 < downs:
                down_copy(step + 1).start()
        now = []
        above = z - 1 - step
        now.append((above, above >= 0))
        if step < downs:
            below = z + 1 + step - nz
            now.append((below, below >= 0))
        for p, there in now:
            pl.when(there)(functools.partial(exchange, p))
        order.append(now)
        if step == 3 or step == ups - 2 and ups < 5:
            w_ring(0).wait_recv()
            w_half(0).start()
            w_pair(1).start()
            w_ring(1).wait_recv()
            w_half(1).start()
            w_pair(2).start()
        if step == 5 or step == ups - 1 and ups < 6:
            w_half(0).wait_recv()
            w_half(1).wait_recv()
            w_pair(3).start()
        if step >= 1:
            for p, there in order[step - 1]:
                if there is None:
                    relay(p)
                else:
                    pl.when(there)(functools.partial(relay, p))
    for now in order[ups - 1 :]:
        for p, there in now:
            if there is None:
                relay(p)
            else:
                pl.when(there)(functools.partial(relay, p))
    for step in range(ups):
        up_copy(step).wait_send()
    for step in range(downs):
        down_copy(step).wait_send()
    for side in range(2):
        w_ring(side).wait_send()
        w_half(side).wait_send()
    for which in range(4):
        w_pair(which).wait()
    for now in order:
        for p, there in now:
            if there is None:
                settle(p)
            else:
                pl.when(there)(functools.partial(settle, p))

    def part_copy(to):
        src = att.at[pl.ds(to * rows, rows)]
        dst = abuf.at[:, pl.ds(pl.multiple_of(tp * width, width), width)]
        return remote(src, dst, a_send.at[to], a_recv.at[tp], (kv, to))

    def part_arrival(source):
        src = att.at[pl.ds(0, rows)]
        dst = abuf.at[:, pl.ds(source * width, width)]
        return remote(src, dst, a_send.at[source], a_recv.at[source], (kv, source))

    heads = width // HEAD_DIM
    per_block = ntp // blocks
    lane = lax.broadcasted_iota(jnp.int32, (BLK, width), 1)
    row_id = lax.broadcasted_iota(jnp.int32, (heads * BLK, heads * BLK), 0)
    col_id = lax.broadcasted_iota(jnp.int32, (heads * BLK, heads * BLK), 1)
    logs = []
    for i in range(blocks):
        for j in range(SEL):
            picked[j * BLK : (j + 1) * BLK, :] = pool[idx_ref[i * SEL + j]]
        scores = lax.dot_general(
            q_ref[i],
            picked[:, :width],
            (((1,), (1,)), ((), ())),
            preferred_element_type=jnp.float32,
        )
        scores = scores + bias_ref[i : i + 1, :]
        top = jnp.max(scores, axis=1, keepdims=True)
        weights = jnp.exp(scores - top)
        total = jnp.sum(weights, axis=1, keepdims=True)
        summed = jnp.dot(
            weights.astype(jnp.bfloat16), picked[:, width:], preferred_element_type=jnp.float32
        )
        summed = summed / total
        mixed = summed[:BLK]
        for head in range(1, heads):
            mixed = jnp.where(
                lane // HEAD_DIM == head, summed[head * BLK : (head + 1) * BLK], mixed
            )
        att[i * BLK : (i + 1) * BLK, :] = mixed.astype(jnp.bfloat16)
        for to in range(i * per_block, (i + 1) * per_block):
            @pl.when(to != tp)
            def _():
                part_copy(to).start()

            @pl.when(to == tp)
            def _():
                abuf[:, pl.ds(pl.multiple_of(tp * width, width), width)] = att[
                    to * rows : (to + 1) * rows, :
                ]
        column = top + jnp.log(total)
        logs.append(jnp.sum(jnp.where(row_id == col_id, column, 0.0), axis=0, keepdims=True))
    for head in range(heads):
        lse_ref[head : head + 1, :] = jnp.concatenate(
            [row[:, head * BLK : (head + 1) * BLK] for row in logs], axis=1
        )
    for other in range(ntp):
        @pl.when(other != tp)
        def _():
            part_arrival(other).wait_recv()
            part_copy(other).wait_send()
    total_width = out_ref.shape[1]
    chunk = min(512, total_width)
    for c in range(total_width // chunk):
        cols = slice(c * chunk, (c + 1) * chunk)
        acc = jnp.zeros((rows, chunk), jnp.float32)
        for t in range(ntp):
            acc += jnp.dot(
                abuf[:, t * width : (t + 1) * width],
                wall[t, :, cols],
                preferred_element_type=jnp.float32,
            )
        out_ref[:, cols] = acc.astype(jnp.bfloat16)


def local(nkv, ntp, tokens, w_query, w_key, w_value, w_out, chosen):
    local_rows = tokens.shape[0]
    width = w_query.shape[1]
    heads = width // HEAD_DIM
    blocks = local_rows // BLK
    nz = nkv // NY
    device = lax.axis_index("kv")
    z, y = device // NY, device % NY
    vmem = pl.BlockSpec(memory_space=pltpu.VMEM)
    smem = pl.BlockSpec(memory_space=pltpu.SMEM)
    positions = device * local_rows + jnp.arange(local_rows)
    cos_part, sin_part = rotary_tables(positions, width)
    kv_here, query = pl.pallas_call(
        project,
        out_shape=(
            jax.ShapeDtypeStruct((blocks, BLK, 2 * width), jnp.bfloat16),
            jax.ShapeDtypeStruct((blocks, heads * BLK, width), jnp.bfloat16),
        ),
        in_specs=[vmem] * 6,
        out_specs=(vmem, vmem),
        compiler_params=pltpu.CompilerParams(vmem_limit_bytes=24 * 1024 * 1024),
    )(tokens, w_query, w_key, w_value, cos_part, sin_part)

    plane_lists = lax.dynamic_slice_in_dim(chosen, z * NY * blocks, NY * blocks, 0)
    plane_lists = plane_lists.reshape(NY, blocks * SEL)
    every = jnp.arange(chosen.shape[0])
    wanted = jnp.any(plane_lists[:, :, None] == every[None, None, :], axis=1)
    wanted = wanted.reshape(NY, nz, NY, blocks)
    order = jnp.arange(blocks)
    lowest = jnp.min(jnp.where(wanted, order, blocks - 1), axis=-1)
    highest = jnp.max(jnp.where(wanted, order, 0), axis=-1)
    table = jnp.stack([lowest, highest], axis=-1)
    dest = (y + 1 + jnp.arange(NY - 1)) % NY
    sent = jnp.take(jnp.take(table, y, axis=2), dest, axis=0)
    sel = jnp.transpose(sent, (1, 0, 2)).reshape(-1)

    own_lists = lax.dynamic_slice_in_dim(chosen, device * blocks, blocks, 0)
    usable = own_lists >= 0
    entry = jnp.where(usable, own_lists, device * blocks)
    source = entry // blocks
    from_z, from_y, block = source // NY, source % NY, entry % blocks
    low_mine = jnp.take(lowest, y, axis=0)
    second = (block != low_mine[from_z, from_y]).astype(jnp.int32)
    ahead = (from_y - y) % NY
    left_base = nz * blocks
    right_base = left_base + 3 * nz
    far_base = right_base + 3 * nz
    place = jnp.where(
        ahead == 0,
        from_z * blocks + block,
        jnp.where(
            ahead == NY - 1,
            left_base + 3 * from_z + second,
            jnp.where(ahead == 1, right_base + 3 * from_z + second, far_base + second * nz + from_z),
        ),
    )
    idx = place.reshape(-1).astype(jnp.int32)
    bias = jnp.where(usable, 0.0, MASKED)
    bias = jnp.broadcast_to(bias[:, :, None], (blocks, SEL, BLK)).reshape(blocks, SEL * BLK)

    ups = nz // 2
    out_rows = local_rows // ntp
    dma = pltpu.SemaphoreType.DMA
    pool_size = far_base + 2 * nz
    return pl.pallas_call(
        functools.partial(attend, nz, ntp),
        out_shape=(
            jax.ShapeDtypeStruct((out_rows, w_out.shape[1]), jnp.bfloat16),
            jax.ShapeDtypeStruct((heads, local_rows), jnp.float32),
        ),
        in_specs=[vmem] * 4 + [smem] * 2,
        out_specs=(vmem, vmem),
        scratch_shapes=[
            pltpu.VMEM((pool_size, BLK, 2 * width), jnp.bfloat16),
            pltpu.VMEM((nz, 3, BLK, 2 * width), jnp.bfloat16),
            pltpu.VMEM((nz, 3, BLK, 2 * width), jnp.bfloat16),
            pltpu.VMEM((SEL * BLK, 2 * width), jnp.bfloat16),
            pltpu.VMEM((ntp, width, w_out.shape[1]), jnp.bfloat16),
            pltpu.VMEM((local_rows, width), jnp.bfloat16),
            pltpu.VMEM((out_rows, ntp * width), jnp.bfloat16),
            dma((ups,)),
            dma((ups,)),
            dma((ups,)),
            dma((ups,)),
        ]
        + [dma((nz,))] * 8
        + [dma((8,))] * 2
        + [dma((ntp,))] * 2,
        compiler_params=pltpu.CompilerParams(
            collective_id=0, has_side_effects=True, vmem_limit_bytes=48 * 1024 * 1024
        ),
    )(kv_here, query, w_out, bias, sel, idx)


def solution(mesh):
    placed = (P("kv", None), P(None, "tp"), P(None, "tp"), P(None, "tp"), P("tp", None), P())
    return jax.shard_map(
        functools.partial(local, mesh.shape["kv"], mesh.shape["tp"]),
        mesh=mesh,
        in_specs=placed,
        out_specs=(P(("kv", "tp"), None), P("tp", "kv")),
        check_vma=False,
    )
```

time: 271 us -> 77.6 us (0.29)
  the two profiles are of different devices: /device:TPU:1 before, /device:TPU:487 now
where the time goes in v1:
time: 77.6 us; the launch traced here: 77.3 us
  Pallas kernels  65 us (84%)
  local copies, waits for them, and re-layouts  8.52 us (11%)
  other arithmetic  3.11 us (4%)
    pallas_call x1, Pallas kernels, local(): pl.pallas_call(functools.partial(attend, nz, ntp), out_shape=(jax.ShapeDt...  63.9 us
    unnamed x15, local copies, waits for them, and re-layouts  5.67 us
    reduce_min x1, other arithmetic, local(): lowest = jnp.min(jnp.where(wanted, order, blocks - 1), axis=-1)  2.23 us

profile of v1, /device:TPU:487, one launch (start us, length us, event | category | flops | bytes accessed | tf_op | source)
XLA Modules:
  0.0 77.3 jit_solution(16849502197150028420)
XLA Ops:
  0.6 0.0 copy-start
  0.7 0.5 fusion.1
  1.2 0.0 copy-start.1
  1.2 1.2 %copy-done.1 = bf16[256,2048]{1,0:T(8,128)(2,1)S(1)} copy-done((bf16[256,2048]{1,0:T(8,128)(2,1)S(1)}, bf16[256,2048]{1,0:T(8,128)(2,1)}, u32[]{:S(2)}) %copy-start.1) | copy-done | bytes 1048600
  2.4 0.0 copy-start.3
  2.4 1.0 %copy-done.3 = bf16[2048,128]{1,0:T(8,128)(2,1)S(1)} copy-done((bf16[2048,128]{1,0:T(8,128)(2,1)S(1)}, bf16[2048,128]{1,0:T(8,128)(2,1)}, u32[]{:S(2)}) %copy-start.3) | copy-done | bytes 524312
  3.5 0.0 copy-start.4
  3.5 1.0 %copy-done.4 = bf16[2048,128]{1,0:T(8,128)(2,1)S(1)} copy-done((bf16[2048,128]{1,0:T(8,128)(2,1)S(1)}, bf16[2048,128]{1,0:T(8,128)(2,1)}, u32[]{:S(2)}) %copy-start.4) | copy-done | bytes 524312
  4.5 0.0 copy-start.5
  4.5 1.0 %copy-done.5 = bf16[2048,128]{1,0:T(8,128)(2,1)S(1)} copy-done((bf16[2048,128]{1,0:T(8,128)(2,1)S(1)}, bf16[2048,128]{1,0:T(8,128)(2,1)}, u32[]{:S(2)}) %copy-start.5) | copy-done | bytes 524312
  5.6 1.0 %shard_map.77 = (bf16[4,64,256]{2,1,0:T(8,128)(2,1)S(1)}, bf16[4,128,128]{2,1,0:T(8,128)(2,1)S(1)}) custom-call(bf16[256,2048]{1,0:T(8,128)(2,1)S(1)} %copy-done.1, bf16[2048,128]{1,0:T(8,128)(2,1)S(1)} %copy-done.3, bf16[2048,128]{1,0:T(8,128)(2,1)S(1)} %copy-done.4, bf16[2048,128]{1,0:T(8,128)(2,1)S(1)} %copy-done.5, ...), custom_call_target="tpu_custom_call" | custom-call | tf_op jit(solution)/shard_map/pallas_call | solution.py:365
  6.6 0.0 copy-done
  6.6 0.1 constant_dynamic-slice_fusion.1
  6.7 0.1 copy.41
  6.8 0.1 broadcast_in_dim.86
  6.9 0.1 reshape.102.bias_ref
  7.0 0.1 constant_dynamic-slice_fusion
  7.0 0.1 copy.33
  7.1 0.1 eq.36
  7.2 0.1 fusion
  7.3 0.2 reshape.103
  7.5 2.2 %select_reduce_fusion.1 = (s32[4,16,4]{2,1,0:T(8,128)S(1)}, s32[4,16,4]{2,1,0:T(8,128)S(1)}) fusion(pred[4,16,4,4]{3,2,1,0:T(4,128)(4,1)S(1)} %reshape.103), kind=kLoop, calls=%fused_computation.8 | loop fusion | flops 3584 | bytes 3072 | tf_op jit(solution)/shard_map/reduce_min | solution.py:382
  9.7 0.1 copy.35
  9.8 0.1 copy.34
  10.0 0.6 gather_fusion
  10.6 0.1 select_bitcast_fusion
  10.6 0.1 copy.38
  10.7 0.1 reshape.104.sel_ref
  10.9 0.1 copy.39
  11.0 0.1 reshape.178
  11.1 0.0 copy-start.2
  11.1 0.9 %gather_fusion.1 = s32[64]{0:T(128)S(1)} fusion(s32[16,4]{0,1:T(4,128)S(1)} %bitcast.8, s32[64]{0:T(128)S(1)} %reshape.178), kind=kCustom, calls=%fused_computation.1 | custom fusion | bytes 1024 | tf_op jit(solution)/shard_map/gather | solution.py:395
  12.0 0.1 reshape.181
  12.1 0.1 reshape.105.idx_ref
  12.2 0.0 copy-done.2
  12.2 63.9 %shard_map.78 = (bf16[32,2048]{1,0:T(8,128)(2,1)S(1)}, f32[2,256]{1,0:T(2,128)S(1)}) custom-call(bf16[4,64,256]{2,1,0:T(8,128)(2,1)S(1)} %get-tuple-element.4.kv_ref, bf16[4,128,128]{2,1,0:T(8,128)(2,1)S(1)} %get-tuple-element.5.q_ref, bf16[128,2048]{1,0:T(8,128)(2,1)S(1)} %copy-done.2, f32[4,1024]{1,0:T(4,128)S(1)} %reshape.102.bias_ref, ...), custom_call_target="tpu_custom_call" | custom-call | tf_op jit(solution)/shard_map/pallas_call | solution.py:417
  76.1 0.7 copy.44
  76.8 0.6 copy.45
  (10 shorter events, 0.1 us)
Async XLA Ops:
  0.6 6.0 %copy-start = (s32[256,16]{0,1:T(8,128)S(1)}, s32[256,16]{0,1:T(8,128)}, u32[]{:S(2)}) copy-start(s32[256,16]{0,1:T(8,128)} %param.11) | copy-start | bytes 49156
  1.2 1.2 %copy-start.1 = (bf16[256,2048]{1,0:T(8,128)(2,1)S(1)}, bf16[256,2048]{1,0:T(8,128)(2,1)}, u32[]{:S(2)}) copy-start(bf16[256,2048]{1,0:T(8,128)(2,1)} %tokens_ref.1) | copy-start | bytes 3145732
  2.4 1.0 %copy-start.3 = (bf16[2048,128]{1,0:T(8,128)(2,1)S(1)}, bf16[2048,128]{1,0:T(8,128)(2,1)}, u32[]{:S(2)}) copy-start(bf16[2048,128]{1,0:T(8,128)(2,1)} %wq_ref.1) | copy-start | bytes 1572868
  3.5 1.0 %copy-start.4 = (bf16[2048,128]{1,0:T(8,128)(2,1)S(1)}, bf16[2048,128]{1,0:T(8,128)(2,1)}, u32[]{:S(2)}) copy-start(bf16[2048,128]{1,0:T(8,128)(2,1)} %wk_ref.1) | copy-start | bytes 1572868
  4.5 1.0 %copy-start.5 = (bf16[2048,128]{1,0:T(8,128)(2,1)S(1)}, bf16[2048,128]{1,0:T(8,128)(2,1)}, u32[]{:S(2)}) copy-start(bf16[2048,128]{1,0:T(8,128)(2,1)} %wv_ref.1) | copy-start | bytes 1572868
  11.1 1.1 %copy-start.2 = (bf16[128,2048]{1,0:T(8,128)(2,1)S(1)}, bf16[128,2048]{1,0:T(8,128)(2,1)}, u32[]{:S(2)}) copy-start(bf16[128,2048]{1,0:T(8,128)(2,1)} %w_ref.1) | copy-start | bytes 1572868

commit v2 on v1

--- a/solution.py
+++ b/solution.py
@@ -35,36 +35,81 @@
     return values * cos_part + partner * sin_part
 
 
-def project(tokens_ref, wq_ref, wk_ref, wv_ref, cos_ref, sin_ref, kv_ref, q_ref):
-    blocks = kv_ref.shape[0]
-    width = wk_ref.shape[1]
-    cos_part, sin_part = cos_ref[...], sin_ref[...]
-    tokens = tokens_ref[...]
-    keys = jnp.dot(tokens, wk_ref[...], preferred_element_type=jnp.float32)
-    keys = turn(keys, cos_part, sin_part).astype(jnp.bfloat16)
-    kv_ref[:, :, :width] = keys.reshape(blocks, BLK, width)
-    values = jnp.dot(tokens, wv_ref[...], preferred_element_type=jnp.float32).astype(jnp.bfloat16)
-    kv_ref[:, :, width:] = values.reshape(blocks, BLK, width)
-    query = jnp.dot(tokens, wq_ref[...], preferred_element_type=jnp.float32)
-    query = turn(query, cos_part, sin_part).astype(jnp.bfloat16).astype(jnp.float32)
-    query = query * HEAD_DIM ** (-0.5)
-    lane = lax.broadcasted_iota(jnp.int32, query.shape, 1)
-    for head in range(width // HEAD_DIM):
-        mine = jnp.where(lane // HEAD_DIM == head, query, 0.0).astype(jnp.bfloat16)
-        q_ref[:, head * BLK : (head + 1) * BLK, :] = mine.reshape(blocks, BLK, width)
+def make_tables(nz, blocks, kv, chosen_ref, table):
+    z, y = kv // NY, kv % NY
+    row = lax.broadcasted_iota(jnp.int32, table.shape[1:], 0)
+    lane = lax.broadcasted_iota(jnp.int32, table.shape[1:], 1)
+    found = jnp.zeros(table.shape[1:], jnp.int32)
+    target = lax.broadcasted_iota(jnp.int32, (nz, SEL), 0) * (NY * blocks) + y * blocks
+    for ahead in range(1, NY):
+        dest = z * NY + (y + ahead) % NY
+        rows = [chosen_ref[pl.ds(dest * blocks + r, 1), :] for r in range(blocks)]
+        low = jnp.full((nz, 1), blocks - 1, jnp.int32)
+        high = jnp.zeros((nz, 1), jnp.int32)
+        hits = []
+        for b in range(blocks):
+            hit = jnp.zeros((nz, SEL), jnp.int32)
+            for entries in rows:
+                hit = jnp.where(entries == target + b, 1, hit)
+            hits.append(jnp.max(hit, axis=1, keepdims=True))
+        for b in range(blocks):
+            high = jnp.where(hits[b] > 0, b, high)
+            low = jnp.where(hits[blocks - 1 - b] > 0, blocks - 1 - b, low)
+        found = jnp.where(lane == (ahead - 1) * 2, low, found)
+        found = jnp.where(lane == (ahead - 1) * 2 + 1, high, found)
+    table[0] = found
+    size = blocks * SEL
+    mine = jnp.concatenate(
+        [chosen_ref[pl.ds(kv * blocks + r, 1), :] for r in range(blocks)], axis=1
+    )
+    mine = jnp.where(mine >= 0, mine, kv * blocks)
+    across = jnp.broadcast_to(mine, (size, size))
+    diagonal = lax.broadcasted_iota(jnp.int32, (size, size), 0) == lax.broadcasted_iota(
+        jnp.int32, (size, size), 1
+    )
+    down = jnp.sum(jnp.where(diagonal, across, 0), axis=1, keepdims=True)
+    lower = (down // blocks == across // blocks) & (down < across)
+    second = jnp.max(jnp.where(lower, 1, 0), axis=0, keepdims=True)
+    source = mine // blocks
+    from_z, ahead = source // NY, (source % NY - y + NY) % NY
+    left_base = nz * blocks
+    right_base = left_base + 3 * nz
+    far_base = right_base + 3 * nz
+    place = jnp.where(
+        ahead == 0,
+        mine % blocks + from_z * blocks,
+        jnp.where(
+            ahead == NY - 1,
+            left_base + 3 * from_z + second,
+            jnp.where(ahead == 1, right_base + 3 * from_z + second, far_base + second * nz + from_z),
+        ),
+    )
+    full = jnp.concatenate([place, jnp.zeros((1, table.shape[2] - size), jnp.int32)], axis=1)
+    table[1] = jnp.broadcast_to(full, table.shape[1:])
 
 
 def attend(
     nz,
     ntp,
-    kv_ref,
+    tokens_hbm,
+    wq_hbm,
+    wk_hbm,
+    wv_hbm,
+    w_hbm,
+    chosen_ref,
+    cos_ref,
+    sin_ref,
+    out_ref,
+    lse_ref,
+    tokens_ref,
+    wq_ref,
+    wk_ref,
+    wv_ref,
     q_ref,
-    w_ref,
-    bias_ref,
+    table,
     sel_ref,
     idx_ref,
-    out_ref,
-    lse_ref,
+    local_sem,
     pool,
     to_right,
     to_left,
@@ -101,13 +146,27 @@
     x_right = ((x + 1) % nx) * 2 + core
     x_left = ((x + nx - 1) % nx) * 2 + core
     partner = x * 2 + (1 - core)
-    blocks = kv_ref.shape[0]
-    width = w_ref.shape[0]
+    width = wk_ref.shape[1]
+    blocks = att.shape[0] // BLK
+    heads = width // HEAD_DIM
     left_base = nz * blocks
     right_base = left_base + 3 * nz
     far0_base = right_base + 3 * nz
     far1_base = far0_base + nz
     rows = att.shape[0] // ntp
+
+    def load(which, src, dst):
+        return pltpu.make_async_copy(src, dst, local_sem.at[which])
+
+    loads = [
+        load(0, tokens_hbm, tokens_ref),
+        load(1, wk_hbm, wk_ref),
+        load(2, wv_hbm, wv_ref),
+        load(3, w_hbm, wall.at[tp]),
+        load(4, wq_hbm, wq_ref),
+    ]
+    for copy in loads:
+        copy.start()
 
     barrier = pltpu.get_barrier_semaphore()
     for peer in (up, down, right, left):
@@ -116,6 +175,10 @@
         pl.semaphore_signal(
             barrier, inc=1, device_id=(kv, (tp + step) % ntp), device_id_type=MESH
         )
+    make_tables(nz, blocks, kv, chosen_ref, table)
+    to_smem = [load(5, table.at[0], sel_ref), load(6, table.at[1, pl.ds(0, 8)], idx_ref)]
+    for copy in to_smem:
+        copy.start()
     pl.semaphore_wait(barrier, 4 + ntp - 1)
 
     def remote(src, dst, send, recv, device):
@@ -131,18 +194,15 @@
     ups = (nz - 1 + 1) // 2
     downs = nz - 1 - ups
 
-    def plane(p):
-        return pool.at[pl.ds(p * blocks, blocks)]
-
-    def up_copy(step):
-        p = (z + nz - step) % nz
-        src = kv_ref if step == 0 else plane(p)
-        return remote(src, plane(p), up_send.at[step], up_recv.at[step], (up, tp))
-
-    def down_copy(step):
-        p = (z + step) % nz
-        src = kv_ref if step == 0 else plane(p)
-        return remote(src, plane(p), dn_send.at[step], dn_recv.at[step], (down, tp))
+    def up_copy(step, b):
+        at = pool.at[(z + nz - step) % nz * blocks + b]
+        sem = step * blocks + b
+        return remote(at, at, up_send.at[sem], up_recv.at[sem], (up, tp))
+
+    def down_copy(step, b):
+        at = pool.at[(z + step) % nz * blocks + b]
+        sem = step * blocks + b
+        return remote(at, at, dn_send.at[sem], dn_recv.at[sem], (down, tp))
 
     def right_copy(p):
         dst = pool.at[pl.ds(left_base + 3 * p, 3)]
@@ -164,7 +224,7 @@
         here = [pool[p * blocks + b] for b in range(blocks)]
 
         def pick(ahead, c):
-            which = sel_ref[(p * 3 + ahead - 1) * 2 + c]
+            which = sel_ref[p, (ahead - 1) * 2 + c]
             found = here[blocks - 1]
             for b in range(blocks - 1):
                 found = jnp.where(which == b, here[b], found)
@@ -194,9 +254,8 @@
     half = width // 2
 
     def w_ring(side):
-        src = w_ref
         peer = x_right if side == 0 else x_left
-        return remote(src, wall.at[tp], w_send.at[side], w_recv.at[side], (kv, peer))
+        return remote(wall.at[tp], wall.at[tp], w_send.at[side], w_recv.at[side], (kv, peer))
 
     def w_half(side):
         origin = x_left if side == 0 else x_right
@@ -207,27 +266,47 @@
     def w_pair(which):
         far = ((x + 2) % nx) * 2 + core
         owner = (tp, x_left, x_right, far)[which]
-        src = w_ref if which == 0 else wall.at[owner]
-        return remote(src, wall.at[owner], w_send.at[4 + which], w_recv.at[4 + which], (kv, partner))
-
-    up_copy(0).start()
-    down_copy(0).start()
+        return remote(wall.at[owner], wall.at[owner], w_send.at[4 + which], w_recv.at[4 + which], (kv, partner))
+
+    loads[0].wait()
+    loads[1].wait()
+    cos_part, sin_part = cos_ref[...], sin_ref[...]
+    keys = jnp.dot(tokens_ref[...], wk_ref[...], preferred_element_type=jnp.float32)
+    keys = turn(keys, cos_part, sin_part).astype(jnp.bfloat16)
+    pool[pl.ds(z * blocks, blocks), :, :width] = keys.reshape(blocks, BLK, width)
+    loads[2].wait()
+    values = jnp.dot(tokens_ref[...], wv_ref[...], preferred_element_type=jnp.float32)
+    values = values.astype(jnp.bfloat16)
+    pool[pl.ds(z * blocks, blocks), :, width:] = values.reshape(blocks, BLK, width)
+    for b in range(blocks):
+        up_copy(0, b).start()
+        down_copy(0, b).start()
+    for copy in to_smem:
+        copy.wait()
+    exchange(z)
+    loads[3].wait()
     w_ring(0).start()
     w_ring(1).start()
     w_pair(0).start()
-    pool[pl.ds(z * blocks, blocks)] = kv_ref[...]
-    wall[tp] = w_ref[...]
-    exchange(z)
+    loads[4].wait()
+    query = jnp.dot(tokens_ref[...], wq_ref[...], preferred_element_type=jnp.float32)
+    query = turn(query, cos_part, sin_part).astype(jnp.bfloat16).astype(jnp.float32)
+    query = query * HEAD_DIM ** (-0.5)
+    channel = lax.broadcasted_iota(jnp.int32, query.shape, 1)
+    for head in range(heads):
+        mine = jnp.where(channel // HEAD_DIM == head, query, 0.0).astype(jnp.bfloat16)
+        q_ref[:, head * BLK : (head + 1) * BLK, :] = mine.reshape(blocks, BLK, width)
 
     order = [[(z, None)]]
     for step in range(ups):
-        up_copy(step).wait_recv()
-        if step + 1 < ups:
-            up_copy(step + 1).start()
-        if step < downs:
-            down_copy(step).wait_recv()
-            if step + 1 < downs:
-                down_copy(step + 1).start()
+        for b in range(blocks):
+            up_copy(step, b).wait_recv()
+            if step + 1 < ups:
+                up_copy(step + 1, b).start()
+            if step < downs:
+                down_copy(step, b).wait_recv()
+                if step + 1 < downs:
+                    down_copy(step + 1, b).start()
         now = []
         above = z - 1 - step
         now.append((above, above >= 0))
@@ -260,10 +339,11 @@
                 relay(p)
             else:
                 pl.when(there)(functools.partial(relay, p))
-    for step in range(ups):
-        up_copy(step).wait_send()
-    for step in range(downs):
-        down_copy(step).wait_send()
+    for b in range(blocks):
+        for step in range(ups):
+            up_copy(step, b).wait_send()
+        for step in range(downs):
+            down_copy(step, b).wait_send()
     for side in range(2):
         w_ring(side).wait_send()
         w_half(side).wait_send()
@@ -286,22 +366,24 @@
         dst = abuf.at[:, pl.ds(source * width, width)]
         return remote(src, dst, a_send.at[source], a_recv.at[source], (kv, source))
 
-    heads = width // HEAD_DIM
     per_block = ntp // blocks
     lane = lax.broadcasted_iota(jnp.int32, (BLK, width), 1)
     row_id = lax.broadcasted_iota(jnp.int32, (heads * BLK, heads * BLK), 0)
     col_id = lax.broadcasted_iota(jnp.int32, (heads * BLK, heads * BLK), 1)
+    key_id = lax.broadcasted_iota(jnp.int32, (1, SEL * BLK), 1)
     logs = []
     for i in range(blocks):
         for j in range(SEL):
-            picked[j * BLK : (j + 1) * BLK, :] = pool[idx_ref[i * SEL + j]]
+            picked[j * BLK : (j + 1) * BLK, :] = pool[idx_ref[0, i * SEL + j]]
         scores = lax.dot_general(
             q_ref[i],
             picked[:, :width],
             (((1,), (1,)), ((), ())),
             preferred_element_type=jnp.float32,
         )
-        scores = scores + bias_ref[i : i + 1, :]
+        listed = chosen_ref[pl.ds(kv * blocks + i, 1), :]
+        count = jnp.sum((listed >= 0).astype(jnp.int32), axis=1, keepdims=True)
+        scores = jnp.where(key_id < count * BLK, scores, MASKED)
         top = jnp.max(scores, axis=1, keepdims=True)
         weights = jnp.exp(scores - top)
         total = jnp.sum(weights, axis=1, keepdims=True)
@@ -357,72 +439,32 @@
     blocks = local_rows // BLK
     nz = nkv // NY
     device = lax.axis_index("kv")
-    z, y = device // NY, device % NY
     vmem = pl.BlockSpec(memory_space=pltpu.VMEM)
-    smem = pl.BlockSpec(memory_space=pltpu.SMEM)
+    hbm = pl.BlockSpec(memory_space=pl.ANY)
     positions = device * local_rows + jnp.arange(local_rows)
     cos_part, sin_part = rotary_tables(positions, width)
-    kv_here, query = pl.pallas_call(
-        project,
-        out_shape=(
-            jax.ShapeDtypeStruct((blocks, BLK, 2 * width), jnp.bfloat16),
-            jax.ShapeDtypeStruct((blocks, heads * BLK, width), jnp.bfloat16),
-        ),
-        in_specs=[vmem] * 6,
-        out_specs=(vmem, vmem),
-        compiler_params=pltpu.CompilerParams(vmem_limit_bytes=24 * 1024 * 1024),
-    )(tokens, w_query, w_key, w_value, cos_part, sin_part)
-
-    plane_lists = lax.dynamic_slice_in_dim(chosen, z * NY * blocks, NY * blocks, 0)
-    plane_lists = plane_lists.reshape(NY, blocks * SEL)
-    every = jnp.arange(chosen.shape[0])
-    wanted = jnp.any(plane_lists[:, :, None] == every[None, None, :], axis=1)
-    wanted = wanted.reshape(NY, nz, NY, blocks)
-    order = jnp.arange(blocks)
-    lowest = jnp.min(jnp.where(wanted, order, blocks - 1), axis=-1)
-    highest = jnp.max(jnp.where(wanted, order, 0), axis=-1)
-    table = jnp.stack([lowest, highest], axis=-1)
-    dest = (y + 1 + jnp.arange(NY - 1)) % NY
-    sent = jnp.take(jnp.take(table, y, axis=2), dest, axis=0)
-    sel = jnp.transpose(sent, (1, 0, 2)).reshape(-1)
-
-    own_lists = lax.dynamic_slice_in_dim(chosen, device * blocks, blocks, 0)
-    usable = own_lists >= 0
-    entry = jnp.where(usable, own_lists, device * blocks)
-    source = entry // blocks
-    from_z, from_y, block = source // NY, source % NY, entry % blocks
-    low_mine = jnp.take(lowest, y, axis=0)
-    second = (block != low_mine[from_z, from_y]).astype(jnp.int32)
-    ahead = (from_y - y) % NY
-    left_base = nz * blocks
-    right_base = left_base + 3 * nz
-    far_base = right_base + 3 * nz
-    place = jnp.where(
-        ahead == 0,
-        from_z * blocks + block,
-        jnp.where(
-            ahead == NY - 1,
-            left_base + 3 * from_z + second,
-            jnp.where(ahead == 1, right_base + 3 * from_z + second, far_base + second * nz + from_z),
-        ),
-    )
-    idx = place.reshape(-1).astype(jnp.int32)
-    bias = jnp.where(usable, 0.0, MASKED)
-    bias = jnp.broadcast_to(bias[:, :, None], (blocks, SEL, BLK)).reshape(blocks, SEL * BLK)
-
     ups = nz // 2
     out_rows = local_rows // ntp
     dma = pltpu.SemaphoreType.DMA
-    pool_size = far_base + 2 * nz
+    pool_size = nz * (blocks + 8)
     return pl.pallas_call(
         functools.partial(attend, nz, ntp),
         out_shape=(
             jax.ShapeDtypeStruct((out_rows, w_out.shape[1]), jnp.bfloat16),
             jax.ShapeDtypeStruct((heads, local_rows), jnp.float32),
         ),
-        in_specs=[vmem] * 4 + [smem] * 2,
+        in_specs=[hbm] * 5 + [vmem] * 3,
         out_specs=(vmem, vmem),
         scratch_shapes=[
+            pltpu.VMEM(tokens.shape, jnp.bfloat16),
+            pltpu.VMEM(w_query.shape, jnp.bfloat16),
+            pltpu.VMEM(w_key.shape, jnp.bfloat16),
+            pltpu.VMEM(w_value.shape, jnp.bfloat16),
+            pltpu.VMEM((blocks, heads * BLK, width), jnp.bfloat16),
+            pltpu.VMEM((2, nz, 128), jnp.int32),
+            pltpu.SMEM((nz, 128), jnp.int32),
+            pltpu.SMEM((8, 128), jnp.int32),
+            dma((7,)),
             pltpu.VMEM((pool_size, BLK, 2 * width), jnp.bfloat16),
             pltpu.VMEM((nz, 3, BLK, 2 * width), jnp.bfloat16),
             pltpu.VMEM((nz, 3, BLK, 2 * width), jnp.bfloat16),
@@ -430,18 +472,15 @@
             pltpu.VMEM((ntp, width, w_out.shape[1]), jnp.bfloat16),
             pltpu.VMEM((local_rows, width), jnp.bfloat16),
             pltpu.VMEM((out_rows, ntp * width), jnp.bfloat16),
-            dma((ups,)),
-            dma((ups,)),
-            dma((ups,)),
-            dma((ups,)),
         ]
+        + [dma((ups * blocks,))] * 4
         + [dma((nz,))] * 8
         + [dma((8,))] * 2
         + [dma((ntp,))] * 2,
         compiler_params=pltpu.CompilerParams(
-            collective_id=0, has_side_effects=True, vmem_limit_bytes=48 * 1024 * 1024
+            collective_id=0, has_side_effects=True, vmem_limit_bytes=56 * 1024 * 1024
         ),
-    )(kv_here, query, w_out, bias, sel, idx)
+    )(tokens, w_query, w_key, w_value, w_out, chosen, cos_part, sin_part)
 
 
 def solution(mesh):

time: 77.6 us -> 71.9 us (0.927)
  local copies, waits for them, and re-layouts: 8.52 us -> 3.58 us
  other arithmetic: 3.11 us -> 1.25 us
  Pallas kernels: 65 us -> 66.2 us
    pallas_call x1, Pallas kernels: 63.9 us -> 66.2 us  [local(): pl.pallas_call(functools.partial(attend, nz, ntp), out_shape=(jax.ShapeDt...]
    reduce_min x1 -> x0, other arithmetic: 2.23 us -> none  [local(): lowest = jnp.min(jnp.where(wanted, order, blocks - 1), axis=-1)]
    unnamed x15 -> x7, local copies, waits for them, and re-layouts: 5.67 us -> 3.58 us
    gather x3 -> x0, local copies, waits for them, and re-layouts: 1.54 us -> none  [the longest x2 0.97 us: local(): second = (block != low_mine[from_z, from_y]).astype(jnp.int32)]
    pallas_call x1 -> x0, Pallas kernels: 1.04 us -> none  [local(): pl.pallas_call(project, out_shape=(jax.ShapeDtypeStruct((blocks, BLK, 2 *...]
where the time goes in v2:
time: 71.9 us; the launch traced here: 71.7 us
  Pallas kernels  66.2 us (92%)
  local copies, waits for them, and re-layouts  3.58 us (5%)
  other arithmetic  1.25 us (2%)
    pallas_call x1, Pallas kernels, local(): pl.pallas_call(functools.partial(attend, nz, ntp), out_shape=(jax.ShapeDt...  66.2 us
    unnamed x7, local copies, waits for them, and re-layouts  3.58 us

profile of v2, /device:TPU:487, one launch (start us, length us, event | category | flops | bytes accessed | tf_op | source)
XLA Modules:
  0.0 71.7 jit_solution(6958150024782923270)
XLA Ops:
  0.6 0.0 copy-start
  0.7 0.7 copy-done
  1.3 0.8 %copy.8.chosen_ref = s32[256,16]{1,0:T(8,128)} copy(s32[256,16]{0,1:T(8,128)S(1)} %copy-done) | data formatting | bytes 32768 | tf_op args[5]
  2.1 1.2 %fusion = (f32[256,128]{1,0:T(8,128)}, f32[256,128]{1,0:T(8,128)}) fusion(f32[128]{0:T(128)S(1)} %get-tuple-element.4, f32[128]{0:T(128)S(1)} %get-tuple-element.5, f32[256]{0:T(256)S(1)} %add_convert_fusion), kind=kLoop, calls=%fused_computation.2 | loop fusion | flops 65536 | bytes 264192 | tf_op jit(solution)/shard_map/mul | solution.py:25
  3.3 66.2 %shard_map.77 = (bf16[32,2048]{1,0:T(8,128)(2,1)}, f32[2,256]{1,0:T(2,128)}) custom-call(bf16[256,2048]{1,0:T(8,128)(2,1)} %tokens_hbm.1, bf16[2048,128]{1,0:T(8,128)(2,1)} %wq_hbm.1, bf16[2048,128]{1,0:T(8,128)(2,1)} %wk_hbm.1, bf16[2048,128]{1,0:T(8,128)(2,1)} %wv_hbm.1, bf16[128,2048]{1,0:T(8,128)(2,1)} %w_hbm.1, s32[256,16]{1,0:T(8,128)} %copy.8.chosen_ref, ...), custom_call_target="tpu_custom_call" | custom-call | tf_op jit(solution)/shard_map/pallas_call | solution.py:450
  69.6 0.0 copy-start.1
  69.6 1.6 %copy.11 = bf16[32,2048]{1,0:T(8,128)(2,1)} copy(bf16[32,2048]{1,0:T(8,128)(2,1)} %get-tuple-element.8) | data formatting | bytes 262144
  71.1 0.0 copy-done.1
  71.1 0.6 copy.12
  (2 shorter events, 0.0 us)
Async XLA Ops:
  0.6 0.7 %copy-start = (s32[256,16]{0,1:T(8,128)S(1)}, s32[256,16]{0,1:T(8,128)}, u32[]{:S(2)}) copy-start(s32[256,16]{0,1:T(8,128)} %param.11) | copy-start | bytes 49156
  69.6 1.6 %copy-start.1 = (f32[2,256]{1,0:T(2,128)S(1)}, f32[2,256]{1,0:T(2,128)}, u32[]{:S(2)}) copy-start(f32[2,256]{1,0:T(2,128)} %get-tuple-element.9) | copy-start | bytes 6148

commit v3 on v2

--- a/solution.py
+++ b/solution.py
@@ -16,13 +16,29 @@
 MESH = pl.DeviceIdType.MESH
 
 
-def rotary_tables(positions, width):
+def rotary_pieces(first, width):
     half = HEAD_DIM // 2
     lane = jnp.arange(width)
     inverse = ROTARY_BASE ** (-(lane % half).astype(jnp.float32) / half)
-    angles = positions.astype(jnp.float32)[:, None] * inverse[None, :]
+    row = jnp.arange(40)
+    position = jnp.where(row < 16, 16 * row, jnp.where(row < 32, row - 16, first))
+    angles = position.astype(jnp.float32)[:, None] * inverse[None, :]
+    return jnp.cos(angles), jnp.sin(angles)
+
+
+def rotary_tables(cos_piece, sin_piece, cos_ref, sin_ref):
+    half = HEAD_DIM // 2
+    cos_first, sin_first = cos_piece[32:33, :], sin_piece[32:33, :]
+    cos_tens, sin_tens = cos_piece[:16, :], sin_piece[:16, :]
+    cos_ones, sin_ones = cos_piece[16:32, :], sin_piece[16:32, :]
+    lane = lax.broadcasted_iota(jnp.int32, cos_ones.shape, 1)
     sign = jnp.where(lane % HEAD_DIM < half, -1.0, 1.0)
-    return jnp.cos(angles), jnp.sin(angles) * sign[None, :]
+    cos_row = cos_first * cos_tens - sin_first * sin_tens
+    sin_row = sin_first * cos_tens + cos_first * sin_tens
+    for t in range(cos_ref.shape[0] // 16):
+        c, n = cos_row[t : t + 1, :], sin_row[t : t + 1, :]
+        cos_ref[t * 16 : (t + 1) * 16, :] = c * cos_ones - n * sin_ones
+        sin_ref[t * 16 : (t + 1) * 16, :] = (n * cos_ones + c * sin_ones) * sign
 
 
 def turn(values, cos_part, sin_part):
@@ -96,9 +112,9 @@
     wk_hbm,
     wv_hbm,
     w_hbm,
-    chosen_ref,
-    cos_ref,
-    sin_ref,
+    chosen_hbm,
+    cos_piece,
+    sin_piece,
     out_ref,
     lse_ref,
     tokens_ref,
@@ -106,6 +122,10 @@
     wk_ref,
     wv_ref,
     q_ref,
+    chosen_across,
+    chosen_ref,
+    cos_ref,
+    sin_ref,
     table,
     sel_ref,
     idx_ref,
@@ -117,18 +137,11 @@
     wall,
     att,
     abuf,
-    up_send,
-    up_recv,
-    dn_send,
-    dn_recv,
-    rs_send,
-    rs_recv,
-    ls_send,
-    ls_recv,
-    rf_send,
-    rf_recv,
-    lf_send,
-    lf_recv,
+    z_send,
+    z_recv,
+    y_send,
+    y_recv,
+    relay_recv,
     w_send,
     w_recv,
     a_send,
@@ -165,6 +178,8 @@
         load(3, w_hbm, wall.at[tp]),
         load(4, wq_hbm, wq_ref),
     ]
+    listing = load(7, chosen_hbm, chosen_across)
+    listing.start()
     for copy in loads:
         copy.start()
 
@@ -175,6 +190,9 @@
         pl.semaphore_signal(
             barrier, inc=1, device_id=(kv, (tp + step) % ntp), device_id_type=MESH
         )
+    rotary_tables(cos_piece, sin_piece, cos_ref, sin_ref)
+    listing.wait()
+    chosen_ref[...] = jnp.transpose(chosen_across[...])
     make_tables(nz, blocks, kv, chosen_ref, table)
     to_smem = [load(5, table.at[0], sel_ref), load(6, table.at[1, pl.ds(0, 8)], idx_ref)]
     for copy in to_smem:
@@ -194,31 +212,41 @@
     ups = (nz - 1 + 1) // 2
     downs = nz - 1 - ups
 
+    part = blocks // 2
+    parts = blocks // part
+
     def up_copy(step, b):
-        at = pool.at[(z + nz - step) % nz * blocks + b]
-        sem = step * blocks + b
-        return remote(at, at, up_send.at[sem], up_recv.at[sem], (up, tp))
+        at = pool.at[pl.ds((z + nz - step) % nz * blocks + b * part, part)]
+        return remote(at, at, z_send, z_recv.at[step * parts + b], (up, tp))
 
     def down_copy(step, b):
-        at = pool.at[(z + step) % nz * blocks + b]
-        sem = step * blocks + b
-        return remote(at, at, dn_send.at[sem], dn_recv.at[sem], (down, tp))
+        at = pool.at[pl.ds((z + step) % nz * blocks + b * part, part)]
+        return remote(at, at, z_send, z_recv.at[step * parts + b], (down, tp))
+
+    def stretch(size):
+        return pool.at[pl.ds(0, size)]
+
+    def arrived(size, sem):
+        remote(stretch(size), stretch(size), z_send, sem, (up, tp)).wait_recv()
+
+    def left_off(size, sem):
+        remote(stretch(size), stretch(size), sem, relay_recv, (up, tp)).wait_send()
 
     def right_copy(p):
         dst = pool.at[pl.ds(left_base + 3 * p, 3)]
-        return remote(to_right.at[p], dst, rs_send.at[p], rs_recv.at[p], (right, tp))
+        return remote(to_right.at[p], dst, y_send, y_recv.at[p], (right, tp))
 
     def left_copy(p):
         dst = pool.at[pl.ds(right_base + 3 * p, 3)]
-        return remote(to_left.at[p], dst, ls_send.at[p], ls_recv.at[p], (left, tp))
+        return remote(to_left.at[p], dst, y_send, y_recv.at[p], (left, tp))
 
     def right_relay(p):
         src = pool.at[left_base + 3 * p + 2]
-        return remote(src, pool.at[far0_base + p], rf_send.at[p], rf_recv.at[p], (right, tp))
+        return remote(src, pool.at[far0_base + p], y_send, relay_recv, (right, tp))
 
     def left_relay(p):
         src = pool.at[right_base + 3 * p + 2]
-        return remote(src, pool.at[far1_base + p], lf_send.at[p], lf_recv.at[p], (left, tp))
+        return remote(src, pool.at[far1_base + p], y_send, relay_recv, (left, tp))
 
     def exchange(p):
         here = [pool[p * blocks + b] for b in range(blocks)]
@@ -240,33 +268,29 @@
         left_copy(p).start()
 
     def relay(p):
-        right_copy(p).wait_recv()
+        arrived(6, y_recv.at[p])
         right_relay(p).start()
-        left_copy(p).wait_recv()
         left_relay(p).start()
-
-    def settle(p):
-        right_relay(p).wait()
-        left_relay(p).wait()
-        right_copy(p).wait_send()
-        left_copy(p).wait_send()
 
     half = width // 2
 
     def w_ring(side):
         peer = x_right if side == 0 else x_left
-        return remote(wall.at[tp], wall.at[tp], w_send.at[side], w_recv.at[side], (kv, peer))
+        return remote(wall.at[tp], wall.at[tp], w_send, w_recv.at[side], (kv, peer))
 
     def w_half(side):
         origin = x_left if side == 0 else x_right
         peer = x_right if side == 0 else x_left
-        part = wall.at[origin, pl.ds(side * half, half)]
-        return remote(part, part, w_send.at[2 + side], w_recv.at[2 + side], (kv, peer))
+        piece = wall.at[origin, pl.ds(side * half, half)]
+        return remote(piece, piece, w_send, w_recv.at[2], (kv, peer))
+
+    def w_arrived(size, sem):
+        remote(wall.at[pl.ds(0, size)], wall.at[pl.ds(0, size)], w_send, sem, (kv, partner)).wait_recv()
 
     def w_pair(which):
         far = ((x + 2) % nx) * 2 + core
         owner = (tp, x_left, x_right, far)[which]
-        return remote(wall.at[owner], wall.at[owner], w_send.at[4 + which], w_recv.at[4 + which], (kv, partner))
+        return remote(wall.at[owner], wall.at[owner], w_send, w_recv.at[3], (kv, partner))
 
     loads[0].wait()
     loads[1].wait()
@@ -278,7 +302,7 @@
     values = jnp.dot(tokens_ref[...], wv_ref[...], preferred_element_type=jnp.float32)
     values = values.astype(jnp.bfloat16)
     pool[pl.ds(z * blocks, blocks), :, width:] = values.reshape(blocks, BLK, width)
-    for b in range(blocks):
+    for b in range(parts):
         up_copy(0, b).start()
         down_copy(0, b).start()
     for copy in to_smem:
@@ -299,14 +323,13 @@
 
     order = [[(z, None)]]
     for step in range(ups):
-        for b in range(blocks):
-            up_copy(step, b).wait_recv()
+        for b in range(parts):
+            both = 2 if step < downs else 1
+            arrived(both * part, z_recv.at[step * parts + b])
             if step + 1 < ups:
                 up_copy(step + 1, b).start()
-            if step < downs:
-                down_copy(step, b).wait_recv()
-                if step + 1 < downs:
-                    down_copy(step + 1, b).start()
+            if step + 1 < downs:
+                down_copy(step + 1, b).start()
         now = []
         above = z - 1 - step
         now.append((above, above >= 0))
@@ -324,8 +347,7 @@
             w_half(1).start()
             w_pair(2).start()
         if step == 5 or step == ups - 1 and ups < 6:
-            w_half(0).wait_recv()
-            w_half(1).wait_recv()
+            w_arrived(1, w_recv.at[2])
             w_pair(3).start()
         if step >= 1:
             for p, there in order[step - 1]:
@@ -339,32 +361,20 @@
                 relay(p)
             else:
                 pl.when(there)(functools.partial(relay, p))
-    for b in range(blocks):
-        for step in range(ups):
-            up_copy(step, b).wait_send()
-        for step in range(downs):
-            down_copy(step, b).wait_send()
-    for side in range(2):
-        w_ring(side).wait_send()
-        w_half(side).wait_send()
-    for which in range(4):
-        w_pair(which).wait()
-    for now in order:
-        for p, there in now:
-            if there is None:
-                settle(p)
-            else:
-                pl.when(there)(functools.partial(settle, p))
+    left_off((ups + downs) * blocks, z_send)
+    w_arrived(4, w_recv.at[3])
+    sent = wall.at[pl.ds(0, ntp - 1)]
+    remote(sent, sent, w_send, w_recv.at[3], (kv, partner)).wait_send()
+    for k in range(nz):
+        @pl.when(z == k)
+        def _():
+            left_off(8 * (k + 1), y_send)
+            arrived(2 * (k + 1), relay_recv)
 
     def part_copy(to):
         src = att.at[pl.ds(to * rows, rows)]
         dst = abuf.at[:, pl.ds(pl.multiple_of(tp * width, width), width)]
-        return remote(src, dst, a_send.at[to], a_recv.at[tp], (kv, to))
-
-    def part_arrival(source):
-        src = att.at[pl.ds(0, rows)]
-        dst = abuf.at[:, pl.ds(source * width, width)]
-        return remote(src, dst, a_send.at[source], a_recv.at[source], (kv, source))
+        return remote(src, dst, a_send, a_recv, (kv, to))
 
     per_block = ntp // blocks
     lane = lax.broadcasted_iota(jnp.int32, (BLK, width), 1)
@@ -413,11 +423,8 @@
         lse_ref[head : head + 1, :] = jnp.concatenate(
             [row[:, head * BLK : (head + 1) * BLK] for row in logs], axis=1
         )
-    for other in range(ntp):
-        @pl.when(other != tp)
-        def _():
-            part_arrival(other).wait_recv()
-            part_copy(other).wait_send()
+    others = abuf.at[:, pl.ds(0, (ntp - 1) * width)]
+    remote(others, others, a_send, a_recv, (kv, partner)).wait()
     total_width = out_ref.shape[1]
     chunk = min(512, total_width)
     for c in range(total_width // chunk):
@@ -432,6 +439,15 @@
         out_ref[:, cols] = acc.astype(jnp.bfloat16)
 
 
+def finish(mixed_ref, log_ref, mixed_out, log_out, sem):
+    first = pltpu.make_async_copy(mixed_ref, mixed_out, sem.at[0])
+    second = pltpu.make_async_copy(log_ref, log_out, sem.at[1])
+    first.start()
+    second.start()
+    first.wait()
+    second.wait()
+
+
 def local(nkv, ntp, tokens, w_query, w_key, w_value, w_out, chosen):
     local_rows = tokens.shape[0]
     width = w_query.shape[1]
@@ -440,20 +456,19 @@
     nz = nkv // NY
     device = lax.axis_index("kv")
     vmem = pl.BlockSpec(memory_space=pltpu.VMEM)
-    hbm = pl.BlockSpec(memory_space=pl.ANY)
-    positions = device * local_rows + jnp.arange(local_rows)
-    cos_part, sin_part = rotary_tables(positions, width)
+    hbm = pl.BlockSpec(memory_space=pltpu.HBM)
+    cos_piece, sin_piece = rotary_pieces(device * local_rows, width)
     ups = nz // 2
     out_rows = local_rows // ntp
     dma = pltpu.SemaphoreType.DMA
     pool_size = nz * (blocks + 8)
-    return pl.pallas_call(
+    mixed, log_sums = pl.pallas_call(
         functools.partial(attend, nz, ntp),
         out_shape=(
             jax.ShapeDtypeStruct((out_rows, w_out.shape[1]), jnp.bfloat16),
             jax.ShapeDtypeStruct((heads, local_rows), jnp.float32),
         ),
-        in_specs=[hbm] * 5 + [vmem] * 3,
+        in_specs=[hbm] * 6 + [vmem] * 2,
         out_specs=(vmem, vmem),
         scratch_shapes=[
             pltpu.VMEM(tokens.shape, jnp.bfloat16),
@@ -461,10 +476,14 @@
             pltpu.VMEM(w_key.shape, jnp.bfloat16),
             pltpu.VMEM(w_value.shape, jnp.bfloat16),
             pltpu.VMEM((blocks, heads * BLK, width), jnp.bfloat16),
+            pltpu.VMEM((SEL, chosen.shape[0]), jnp.int32),
+            pltpu.VMEM((chosen.shape[0], SEL), jnp.int32),
+            pltpu.VMEM((local_rows, width), jnp.float32),
+            pltpu.VMEM((local_rows, width), jnp.float32),
             pltpu.VMEM((2, nz, 128), jnp.int32),
             pltpu.SMEM((nz, 128), jnp.int32),
             pltpu.SMEM((8, 128), jnp.int32),
-            dma((7,)),
+            dma((8,)),
             pltpu.VMEM((pool_size, BLK, 2 * width), jnp.bfloat16),
             pltpu.VMEM((nz, 3, BLK, 2 * width), jnp.bfloat16),
             pltpu.VMEM((nz, 3, BLK, 2 * width), jnp.bfloat16),
@@ -472,15 +491,31 @@
             pltpu.VMEM((ntp, width, w_out.shape[1]), jnp.bfloat16),
             pltpu.VMEM((local_rows, width), jnp.bfloat16),
             pltpu.VMEM((out_rows, ntp * width), jnp.bfloat16),
-        ]
-        + [dma((ups * blocks,))] * 4
-        + [dma((nz,))] * 8
-        + [dma((8,))] * 2
-        + [dma((ntp,))] * 2,
+            dma,
+            dma((2 * ups,)),
+            dma,
+            dma((nz,)),
+            dma,
+            dma,
+            dma((4,)),
+            dma,
+            dma,
+        ],
         compiler_params=pltpu.CompilerParams(
-            collective_id=0, has_side_effects=True, vmem_limit_bytes=56 * 1024 * 1024
+            collective_id=0, has_side_effects=True, vmem_limit_bytes=55000 * 1024
         ),
-    )(tokens, w_query, w_key, w_value, w_out, chosen, cos_part, sin_part)
+    )(tokens, w_query, w_key, w_value, w_out, chosen.T, cos_piece, sin_piece)
+    return pl.pallas_call(
+        finish,
+        out_shape=(
+            jax.ShapeDtypeStruct(mixed.shape, mixed.dtype),
+            jax.ShapeDtypeStruct(log_sums.shape, log_sums.dtype),
+        ),
+        in_specs=[vmem, vmem],
+        out_specs=(hbm, hbm),
+        scratch_shapes=[dma((2,))],
+        compiler_params=pltpu.CompilerParams(vmem_limit_bytes=1024 * 1024),
+    )(mixed, log_sums)
 
 
 def solution(mesh):

time: 71.9 us -> 64.8 us (0.901)
  local copies, waits for them, and re-layouts: 3.58 us -> 0.56 us
  Pallas kernels: 66.2 us -> 63.2 us
  other arithmetic: 1.25 us -> 0.17 us
    pallas_call x1, Pallas kernels: 66.2 us -> 62.5 us  [local(): pl.pallas_call(functools.partial(attend, nz, ntp), out_shape=(jax.ShapeDt...]
    unnamed x7 -> x2, local copies, waits for them, and re-layouts: 3.58 us -> 0.56 us
    mul x1 -> x0, other arithmetic: 1.24 us -> none  [rotary_tables(): return (jnp.cos(angles), jnp.sin(angles) * sign[None, :])]
where the time goes in v3:
time: 64.8 us; the launch traced here: 64.6 us
  Pallas kernels  63.2 us (98%)
  between operations  0.67 us (1%)
    pallas_call x1, Pallas kernels, local(): pl.pallas_call(functools.partial(attend, nz, ntp), out_shape=(jax.ShapeDt...  62.5 us

profile of v3, /device:TPU:487, one launch (start us, length us, event | category | flops | bytes accessed | tf_op | source)
XLA Modules:
  0.0 64.6 jit_solution(3317061678997742173)
XLA Ops:
  0.7 0.0 copy-start
  0.7 0.2 multiply_sine_fusion
  0.8 0.6 copy-done
  1.4 62.5 %shard_map.77 = (bf16[32,2048]{1,0:T(8,128)(2,1)S(1)}, f32[2,256]{1,0:T(2,128)S(1)}) custom-call(bf16[256,2048]{1,0:T(8,128)(2,1)} %tokens_hbm.1, bf16[2048,128]{1,0:T(8,128)(2,1)} %wq_hbm.1, bf16[2048,128]{1,0:T(8,128)(2,1)} %wk_hbm.1, bf16[2048,128]{1,0:T(8,128)(2,1)} %wv_hbm.1, bf16[128,2048]{1,0:T(8,128)(2,1)} %w_hbm.1, s32[16,256]{1,0:T(8,128)S(1)} %bitcast.1, ...), custom_call_target="tpu_custom_call" | custom-call | tf_op jit(solution)/shard_map/pallas_call | solution.py:465
  63.9 0.7 %shard_map.78 = (bf16[32,2048]{1,0:T(8,128)(2,1)}, f32[2,256]{1,0:T(2,128)}) custom-call(bf16[32,2048]{1,0:T(8,128)(2,1)S(1)} %get-tuple-element.4.mixed_ref, f32[2,256]{1,0:T(2,128)S(1)} %get-tuple-element.5.log_ref), custom_call_target="tpu_custom_call" | custom-call | tf_op jit(solution)/shard_map/pallas_call | solution.py:508
  (2 shorter events, 0.0 us)
Async XLA Ops:
  0.7 0.7 %copy-start = (s32[256,16]{0,1:T(8,128)S(1)}, s32[256,16]{0,1:T(8,128)}, u32[]{:S(2)}) copy-start(s32[256,16]{0,1:T(8,128)} %param.11) | copy-start | bytes 49156

commit v4 on v3

v4 whole, which is shorter than its diff:
```python
import functools

import jax
import jax.numpy as jnp
from jax import lax
from jax.experimental import pallas as pl
from jax.experimental.pallas import tpu as pltpu
from jax.sharding import PartitionSpec as P

HEAD_DIM = 64
BLK = 64
SEL = 16
NY = 4
ROTARY_BASE = 500000.0
MASKED = -1e30
MESH = pl.DeviceIdType.MESH


def rotary_pieces(first, width):
    half = HEAD_DIM // 2
    lane = jnp.arange(width)
    inverse = ROTARY_BASE ** (-(lane % half).astype(jnp.float32) / half)
    row = jnp.arange(40)
    position = jnp.where(row < 16, 16 * row, jnp.where(row < 32, row - 16, first))
    angles = position.astype(jnp.float32)[:, None] * inverse[None, :]
    return jnp.cos(angles), jnp.sin(angles)


def rotary_tables(cos_piece, sin_piece, cos_ref, sin_ref):
    half = HEAD_DIM // 2
    cos_first, sin_first = cos_piece[32:33, :], sin_piece[32:33, :]
    cos_tens, sin_tens = cos_piece[:16, :], sin_piece[:16, :]
    cos_ones, sin_ones = cos_piece[16:32, :], sin_piece[16:32, :]
    lane = lax.broadcasted_iota(jnp.int32, cos_ones.shape, 1)
    sign = jnp.where(lane % HEAD_DIM < half, -1.0, 1.0)
    cos_row = cos_first * cos_tens - sin_first * sin_tens
    sin_row = sin_first * cos_tens + cos_first * sin_tens
    for t in range(cos_ref.shape[0] // 16):
        c, n = cos_row[t : t + 1, :], sin_row[t : t + 1, :]
        cos_ref[t * 16 : (t + 1) * 16, :] = c * cos_ones - n * sin_ones
        sin_ref[t * 16 : (t + 1) * 16, :] = (n * cos_ones + c * sin_ones) * sign


def turn(values, cos_part, sin_part):
    width = values.shape[1]
    half = HEAD_DIM // 2
    lane = lax.broadcasted_iota(jnp.int32, values.shape, 1)
    ahead = pltpu.roll(values, width - half, 1)
    behind = pltpu.roll(values, half, 1)
    partner = jnp.where(lane % HEAD_DIM < half, ahead, behind)
    return values * cos_part + partner * sin_part


def make_tables(nz, blocks, kv, dest_z, low, high, planes, chosen_ref, table, at):
    z, y = kv // NY, kv % NY
    lane = lax.broadcasted_iota(jnp.int32, table.shape[1:], 1)
    found = jnp.zeros(table.shape[1:], jnp.int32)
    target = lax.broadcasted_iota(jnp.int32, (nz, SEL), 0) * (NY * blocks) + y * blocks
    for ahead in range(1, NY):
        dest = dest_z * NY + (y + ahead) % NY
        rows = [chosen_ref[pl.ds(dest * blocks + r, 1), :] for r in range(blocks)]
        least = jnp.full((nz, 1), blocks - 1, jnp.int32)
        most = jnp.zeros((nz, 1), jnp.int32)
        hits = []
        for b in range(blocks):
            hit = jnp.zeros((nz, SEL), jnp.int32)
            for entries in rows:
                hit = jnp.where(entries == target + b, 1, hit)
            hits.append(jnp.max(hit, axis=1, keepdims=True))
        for b in range(blocks):
            most = jnp.where(hits[b] > 0, b, most)
            least = jnp.where(hits[blocks - 1 - b] > 0, blocks - 1 - b, least)
        found = jnp.where(lane == (ahead - 1) * 2, least, found)
        found = jnp.where(lane == (ahead - 1) * 2 + 1, most, found)
    table[at] = found
    size = blocks * SEL
    first_row = (dest_z * NY + y) * blocks
    mine = jnp.concatenate([chosen_ref[pl.ds(first_row + r, 1), :] for r in range(blocks)], axis=1)
    across = jnp.broadcast_to(mine, (size, size))
    diagonal = lax.broadcasted_iota(jnp.int32, (size, size), 0) == lax.broadcasted_iota(
        jnp.int32, (size, size), 1
    )
    down = jnp.sum(jnp.where(diagonal, across, 0), axis=1, keepdims=True)
    lower = (down // blocks == across // blocks) & (down >= 0) & (down < across)
    second = jnp.max(jnp.where(lower, 1, 0), axis=0, keepdims=True)
    source = jnp.maximum(mine, 0) // blocks
    from_z, ahead = source // NY, (source % NY - y + NY) % NY
    served = (mine >= 0) & (from_z >= low) & (from_z <= high)
    here = (ahead == 0) | (served == False)
    column = jnp.where(served, from_z * blocks + jnp.maximum(mine, 0) % blocks, z * blocks)
    column = jnp.where(here, column, 0)
    along = jnp.where(
        ahead == NY - 1,
        3 * from_z + second,
        jnp.where(
            ahead == 1,
            3 * planes + 3 * from_z + second,
            6 * planes + second * planes + from_z,
        ),
    )
    along = jnp.where(here, 0, along)
    blank = jnp.zeros((1, table.shape[2] - size), jnp.int32)
    full = [jnp.concatenate([v, blank], axis=1) for v in (column, along, here.astype(jnp.int32))]
    row = lax.broadcasted_iota(jnp.int32, table.shape[1:], 0)
    table[at + 1] = jnp.where(row == 0, full[0], jnp.where(row == 1, full[1], full[2]))


def attend(
    nz,
    ntp,
    tokens_hbm,
    wq_hbm,
    wk_hbm,
    wv_hbm,
    w_hbm,
    chosen_hbm,
    cos_piece,
    sin_piece,
    out_ref,
    lse_ref,
    tokens_ref,
    wq_ref,
    wk_ref,
    wv_ref,
    q_ref,
    q_far,
    chosen_across,
    chosen_ref,
    cos_ref,
    sin_ref,
    table,
    sel_ref,
    idx_ref,
    far_sel_ref,
    far_idx_ref,
    pool,
    own_pool,
    far_pool,
    to_right,
    to_left,
    picked,
    wall,
    mixed_ref,
    wide_ref,
    help_out,
    help_log_out,
    help_in,
    help_log_in,
    att,
    abuf,
    local_sem,
    z_send,
    up_recv,
    down_recv,
    y_send,
    y_recv,
    far_recv,
    relay_recv,
    w_send,
    w_recv,
    help_send,
    help_recv,
    a_send,
    a_recv,
):
    kv = lax.axis_index("kv")
    tp = lax.axis_index("tp")
    z, y = kv // NY, kv % NY
    nx = ntp // 2
    x, core = tp // 2, tp % 2
    up = ((z + 1) % nz) * NY + y
    down = ((z + nz - 1) % nz) * NY + y
    mirror_z = nz - 1 - z
    mirror = mirror_z * NY + y
    right = z * NY + (y + 1) % NY
    left = z * NY + (y + NY - 1) % NY
    x_right = ((x + 1) % nx) * 2 + core
    x_left = ((x + nx - 1) % nx) * 2 + core
    partner = x * 2 + (1 - core)
    width = wk_ref.shape[1]
    blocks = att.shape[0] // BLK
    heads = width // HEAD_DIM
    rows = att.shape[0] // ntp
    ups = nz // 2
    last_far = ups - 2 - z

    def load(which, src, dst):
        return pltpu.make_async_copy(src, dst, local_sem.at[which])

    loads = [
        load(0, tokens_hbm, tokens_ref),
        load(1, wk_hbm, wk_ref),
        load(2, wv_hbm, wv_ref),
        load(3, w_hbm, wall.at[tp]),
        load(4, wq_hbm, wq_ref),
    ]
    listing = load(5, chosen_hbm, chosen_across)
    listing.start()
    for copy in loads:
        copy.start()

    barrier = pltpu.get_barrier_semaphore()
    for peer in (mirror, up, down, right, left):
        pl.semaphore_signal(barrier, inc=1, device_id=(peer, tp), device_id_type=MESH)
    for step in range(1, ntp):
        pl.semaphore_signal(barrier, inc=1, device_id=(kv, (tp + step) % ntp), device_id_type=MESH)
    rotary_tables(cos_piece, sin_piece, cos_ref, sin_ref)
    listing.wait()
    chosen_ref[...] = jnp.transpose(chosen_across[...])
    make_tables(nz, blocks, kv, z, z - ups, nz, nz, chosen_ref, table, 0)
    make_tables(nz, blocks, kv, mirror_z, 0, last_far, nz // 2, chosen_ref, table, 2)
    to_smem = [
        load(5, table.at[0], sel_ref),
        load(6, table.at[1, pl.ds(0, 8)], idx_ref),
        load(7, table.at[2], far_sel_ref),
        load(8, table.at[3, pl.ds(0, 8)], far_idx_ref),
    ]
    for copy in to_smem:
        copy.start()
    pl.semaphore_wait(barrier, 5 + ntp - 1)

    def remote(src, dst, send, recv, device):
        return pltpu.make_async_remote_copy(
            src_ref=src,
            dst_ref=dst,
            send_sem=send,
            recv_sem=recv,
            device_id=device,
            device_id_type=MESH,
        )

    part = blocks // 2
    parts = blocks // part

    def up_copy(step, b):
        at = pool.at[(z + nz - step) % nz * blocks + b]
        return remote(at, at, z_send, up_recv.at[step * blocks + b], (up, tp))

    def down_copy(step, b):
        at = pool.at[pl.ds((z + step) % nz * blocks + b * part, part)]
        return remote(at, at, z_send, down_recv.at[step * parts + b], (down, tp))

    def stretch(size):
        return own_pool.at[pl.ds(0, size)]

    def arrived(size, sem):
        remote(stretch(size), stretch(size), z_send, sem, (up, tp)).wait_recv()

    def left_off(size, sem):
        remote(stretch(size), stretch(size), sem, relay_recv.at[0], (up, tp)).wait_send()

    class Route:
        def __init__(self, kind):
            self.kind = kind
            self.pool = (own_pool, far_pool)[kind]
            self.planes = (nz, nz // 2)[kind]
            self.stage = (0, nz)[kind]
            self.sel = (sel_ref, far_sel_ref)[kind]
            self.recv = (y_recv, far_recv)[kind]

        def right_copy(self, k, p):
            dst = self.pool.at[pl.ds(3 * p, 3)]
            return remote(to_right.at[self.stage + p], dst, y_send, self.recv.at[k], (right, tp))

        def left_copy(self, k, p):
            dst = self.pool.at[pl.ds(3 * self.planes + 3 * p, 3)]
            return remote(to_left.at[self.stage + p], dst, y_send, self.recv.at[k], (left, tp))

        def right_relay(self, p):
            src = self.pool.at[3 * p + 2]
            dst = self.pool.at[6 * self.planes + p]
            return remote(src, dst, y_send, relay_recv.at[self.kind], (right, tp))

        def left_relay(self, p):
            src = self.pool.at[3 * self.planes + 3 * p + 2]
            dst = self.pool.at[7 * self.planes + p]
            return remote(src, dst, y_send, relay_recv.at[self.kind], (left, tp))

        def exchange(self, k, p):
            here = [pool[p * blocks + b] for b in range(blocks)]
            at = self.stage + p

            def pick(ahead, c):
                which = self.sel[p, (ahead - 1) * 2 + c]
                found = here[blocks - 1]
                for b in range(blocks - 1):
                    found = jnp.where(which == b, here[b], found)
                return found

            to_right[at, 0] = pick(1, 0)
            to_right[at, 1] = pick(1, 1)
            to_right[at, 2] = pick(2, 0)
            self.right_copy(k, p).start()
            to_left[at, 0] = pick(3, 0)
            to_left[at, 1] = pick(3, 1)
            to_left[at, 2] = pick(2, 1)
            self.left_copy(k, p).start()

        def relay(self, k, p):
            arrived(6, self.recv.at[k])
            self.right_relay(p).start()
            self.left_relay(p).start()

    routes = (Route(0), Route(1))

    half = width // 2

    def w_ring(side):
        peer = x_right if side == 0 else x_left
        return remote(wall.at[tp], wall.at[tp], w_send, w_recv.at[side], (kv, peer))

    def w_half(side):
        origin = x_left if side == 0 else x_right
        peer = x_right if side == 0 else x_left
        piece = wall.at[origin, pl.ds(side * half, half)]
        return remote(piece, piece, w_send, w_recv.at[2], (kv, peer))

    def w_arrived(size, sem):
        at = wall.at[pl.ds(0, size)]
        remote(at, at, w_send, sem, (kv, partner)).wait_recv()

    def w_pair(which):
        far = ((x + 2) % nx) * 2 + core
        owner = (tp, x_left, x_right, far)[which]
        return remote(wall.at[owner], wall.at[owner], w_send, w_recv.at[3], (kv, partner))

    def w_first():
        w_ring(0).wait_recv()
        w_half(0).start()
        w_pair(1).start()
        w_ring(1).wait_recv()
        w_half(1).start()
        w_pair(2).start()

    def w_second():
        w_arrived(1, w_recv.at[2])
        w_pair(3).start()

    q_copy = remote(q_ref, q_far, help_send.at[0], help_recv.at[0], (mirror, tp))
    o_copy = remote(help_out, help_in, help_send.at[1], help_recv.at[1], (mirror, tp))
    log_copy = remote(help_log_out, help_log_in, help_send.at[2], help_recv.at[2], (mirror, tp))
    helper = last_far >= 0
    helped = mirror_z <= ups - 2

    loads[0].wait()
    loads[1].wait()
    cos_part, sin_part = cos_ref[...], sin_ref[...]
    keys = jnp.dot(tokens_ref[...], wk_ref[...], preferred_element_type=jnp.float32)
    keys = turn(keys, cos_part, sin_part).astype(jnp.bfloat16)
    pool[pl.ds(z * blocks, blocks), :, :width] = keys.reshape(blocks, BLK, width)
    loads[2].wait()
    values = jnp.dot(tokens_ref[...], wv_ref[...], preferred_element_type=jnp.float32)
    values = values.astype(jnp.bfloat16)
    pool[pl.ds(z * blocks, blocks), :, width:] = values.reshape(blocks, BLK, width)

    @pl.when(z < nz - 1)
    def _():
        for b in range(blocks):
            up_copy(0, b).start()

    goes_down = (z >= 1) & (z <= ups - 2)

    @pl.when(goes_down)
    def _():
        for b in range(parts):
            down_copy(0, b).start()

    for copy in to_smem:
        copy.wait()
    pl.when(z <= last_far)(lambda: routes[1].exchange(0, z))
    routes[0].exchange(0, z)
    loads[4].wait()
    query = jnp.dot(tokens_ref[...], wq_ref[...], preferred_element_type=jnp.float32)
    query = turn(query, cos_part, sin_part).astype(jnp.bfloat16).astype(jnp.float32)
    q_ref[...] = (query * HEAD_DIM ** (-0.5)).astype(jnp.bfloat16)
    pl.when(helped)(lambda: q_copy.start())
    loads[3].wait()
    w_ring(0).start()
    w_ring(1).start()
    w_pair(0).start()

    def own_there(k):
        return z - k >= 0

    def far_below(k):
        return (z - k >= 0) & (z - k <= last_far)

    def far_above(step):
        return z + 1 + step <= last_far

    def relay_step(k):
        pl.when(far_below(k))(lambda: routes[1].relay(k, z - k))
        if 1 <= k <= ups - 2:
            pl.when(far_above(k - 1))(lambda: routes[1].relay(ups + k - 1, z + k))
        pl.when(own_there(k))(lambda: routes[0].relay(k, z - k))

    for step in range(ups):
        k = step + 1

        @pl.when(own_there(k))
        def _():
            for b in range(blocks):
                remote(pool.at[b], pool.at[b], z_send, up_recv.at[step * blocks + b], (up, tp)).wait_recv()
                if step + 1 < ups:
                    pl.when(z < nz - 1)(lambda: up_copy(step + 1, b).start())
            pl.when(z - k <= last_far)(lambda: routes[1].exchange(k, z - k))
            routes[0].exchange(k, z - k)

        if step <= ups - 3:

            @pl.when(z + 1 + step <= ups - 2)
            def _():
                for b in range(parts):
                    arrived(part, down_recv.at[step * parts + b])

                    if step <= ups - 4:

                        @pl.when(z >= 1)
                        def _():
                            down_copy(step + 1, b).start()

                pl.when(far_above(step))(lambda: routes[1].exchange(ups + step, z + k))

        if step == 3:
            w_first()
        if step == 5:
            w_second()
        if step >= 1:
            relay_step(step - 1)
    relay_step(ups - 1)
    relay_step(ups)

    def plane_counts(c):
        own = min(c, ups) + 1
        far = max(0, ups - 1 - c)
        ups_sent = min(c, ups - 1) + 1 if c < nz - 1 else 0
        downs_sent = ups - 1 - c if 1 <= c <= ups - 2 else 0
        return own, far, (ups_sent + downs_sent) * blocks

    lane = lax.broadcasted_iota(jnp.int32, (BLK, width), 1)
    wide_lane = lax.broadcasted_iota(jnp.int32, (heads * BLK, width), 1)
    wide_row = lax.broadcasted_iota(jnp.int32, (heads * BLK, width), 0)
    eye = lax.broadcasted_iota(jnp.int32, (heads * BLK, heads * BLK), 0) == lax.broadcasted_iota(
        jnp.int32, (heads * BLK, heads * BLK), 1
    )
    key_block = lax.broadcasted_iota(jnp.int32, (1, SEL * BLK), 1) // BLK

    def by_head(stacked):
        result = stacked[:BLK]
        for head in range(1, heads):
            result = jnp.where(lane // HEAD_DIM == head, stacked[head * BLK : (head + 1) * BLK], result)
        return result

    def attention(i, queries, places, along, dest, low, high):
        for j in range(SEL):
            n = i * SEL + j
            picked[j * BLK : (j + 1) * BLK, :] = jnp.where(
                places[2, n] > 0, pool[places[0, n]], along[places[1, n]]
            )
        rows_here = queries[i * BLK : (i + 1) * BLK, :].astype(jnp.float32)
        stacked = jnp.concatenate([rows_here] * heads, axis=0)
        stacked = jnp.where(wide_lane // HEAD_DIM == wide_row // BLK, stacked, 0.0)
        scores = lax.dot_general(
            stacked.astype(jnp.bfloat16),
            picked[:, :width],
            (((1,), (1,)), ((), ())),
            preferred_element_type=jnp.float32,
        )
        listed = chosen_ref[pl.ds(dest * blocks + i, 1), :]
        block_of = jnp.zeros((1, SEL * BLK), jnp.int32)
        for j in range(SEL):
            block_of = jnp.where(key_block == j, listed[:, j : j + 1], block_of)
        scores = jnp.where((block_of >= low) & (block_of < high), scores, MASKED)
        top = jnp.max(scores, axis=1, keepdims=True)
        weights = jnp.exp(scores - top)
        total = jnp.sum(weights, axis=1, keepdims=True)
        summed = jnp.dot(
            weights.astype(jnp.bfloat16), picked[:, width:], preferred_element_type=jnp.float32
        )
        return by_head(summed / total), top + jnp.log(total)

    first = jnp.maximum(z - ups, 0) * NY * blocks

    def own_attention():
        for c in range(nz):
            pl.when(z == c)(lambda: arrived(2 * plane_counts(c)[0], relay_recv.at[0]))
        for i in range(blocks):
            result, column = attention(i, q_ref, idx_ref, own_pool, kv, first, nz * NY * blocks)
            mixed_ref[i * BLK : (i + 1) * BLK, :] = result
            wide_ref[i * BLK : (i + 1) * BLK, :] = by_head(
                jnp.broadcast_to(column, (heads * BLK, width))
            )

    early = z <= 1
    pl.when(early)(own_attention)

    @pl.when(helper)
    def _():
        for c in range(ups - 1):

            @pl.when(z == c)
            def _():
                arrived(2 * plane_counts(c)[1], relay_recv.at[1])

        q_copy.wait_recv()
        help_log_out[...] = jnp.zeros(help_log_out.shape, jnp.float32)
        limit = (last_far + 1) * NY * blocks
        for i in range(blocks):
            result, column = attention(i, q_far, far_idx_ref, far_pool, mirror, 0, limit)
            help_out[i * BLK : (i + 1) * BLK, :] = result.astype(jnp.bfloat16)
            help_log_out[i : i + 1, :] = jnp.sum(jnp.where(eye, column, 0.0), axis=0, keepdims=True)
        o_copy.start()
        log_copy.start()

    pl.when(z > 1)(own_attention)

    @pl.when(helped)
    def _():
        o_copy.wait_recv()
        log_copy.wait_recv()
        for i in range(blocks):
            at = slice(i * BLK, (i + 1) * BLK)
            row = jnp.broadcast_to(help_log_in[i : i + 1, :], (heads * BLK, width))
            column = jnp.sum(jnp.where(eye, row, 0.0), axis=1, keepdims=True)
            theirs = by_head(jnp.broadcast_to(column, (heads * BLK, width)))
            mine = wide_ref[at, :]
            top = jnp.maximum(mine, theirs)
            share, other = jnp.exp(mine - top), jnp.exp(theirs - top)
            total = share + other
            extra = help_in[at, :].astype(jnp.float32)
            mixed_ref[at, :] = (mixed_ref[at, :] * share + extra * other) / total
            wide_ref[at, :] = top + jnp.log(total)

    def part_copy(to):
        src = att.at[pl.ds(to * rows, rows)]
        dst = abuf.at[:, pl.ds(pl.multiple_of(tp * width, width), width)]
        return remote(src, dst, a_send, a_recv, (kv, to))

    per_block = ntp // blocks
    for i in range(blocks):
        at = slice(i * BLK, (i + 1) * BLK)
        att[at, :] = mixed_ref[at, :].astype(jnp.bfloat16)
        for to in range(i * per_block, (i + 1) * per_block):

            @pl.when(to != tp)
            def _():
                part_copy(to).start()

            @pl.when(to == tp)
            def _():
                abuf[:, pl.ds(pl.multiple_of(tp * width, width), width)] = att[
                    to * rows : (to + 1) * rows, :
                ]

    for head in range(heads):
        cols = slice(head * HEAD_DIM, (head + 1) * HEAD_DIM)
        lse_ref[head : head + 1, :] = jnp.concatenate(
            [
                jnp.sum(
                    jnp.where(
                        eye[:BLK, :HEAD_DIM], wide_ref[i * BLK : (i + 1) * BLK, cols], 0.0
                    ),
                    axis=0,
                    keepdims=True,
                )
                for i in range(blocks)
            ],
            axis=1,
        )

    for c in range(nz):

        @pl.when(z == c)
        def _():
            own, far, sent = plane_counts(c)
            left_off(8 * (own + far), y_send)
            if sent:
                left_off(sent, z_send)

    @pl.when(helper)
    def _():
        o_copy.wait_send()
        log_copy.wait_send()

    pl.when(helped)(lambda: q_copy.wait_send())
    w_arrived(4, w_recv.at[3])
    sent_w = wall.at[pl.ds(0, ntp - 1)]
    remote(sent_w, sent_w, w_send, w_recv.at[3], (kv, partner)).wait_send()
    others = abuf.at[:, pl.ds(0, (ntp - 1) * width)]
    remote(others, others, a_send, a_recv, (kv, partner)).wait()
    total_width = out_ref.shape[1]
    chunk = min(512, total_width)
    for c in range(total_width // chunk):
        cols = slice(c * chunk, (c + 1) * chunk)
        acc = jnp.zeros((rows, chunk), jnp.float32)
        for t in range(ntp):
            acc += jnp.dot(
                abuf[:, t * width : (t + 1) * width],
                wall[t, :, cols],
                preferred_element_type=jnp.float32,
            )
        out_ref[:, cols] = acc.astype(jnp.bfloat16)


def finish(mixed_ref, log_ref, mixed_out, log_out, sem):
    first = pltpu.make_async_copy(mixed_ref, mixed_out, sem.at[0])
    second = pltpu.make_async_copy(log_ref, log_out, sem.at[1])
    first.start()
    second.start()
    first.wait()
    second.wait()


def local(nkv, ntp, tokens, w_query, w_key, w_value, w_out, chosen):
    local_rows = tokens.shape[0]
    width = w_query.shape[1]
    heads = width // HEAD_DIM
    blocks = local_rows // BLK
    nz = nkv // NY
    device = lax.axis_index("kv")
    vmem = pl.BlockSpec(memory_space=pltpu.VMEM)
    hbm = pl.BlockSpec(memory_space=pltpu.HBM)
    cos_piece, sin_piece = rotary_pieces(device * local_rows, width)
    ups = nz // 2
    out_rows = local_rows // ntp
    dma = pltpu.SemaphoreType.DMA
    stage = (nz + ups, 3, BLK, 2 * width)
    bf16, f32, i32 = jnp.bfloat16, jnp.float32, jnp.int32
    mixed, log_sums = pl.pallas_call(
        functools.partial(attend, nz, ntp),
        out_shape=(
            jax.ShapeDtypeStruct((out_rows, w_out.shape[1]), bf16),
            jax.ShapeDtypeStruct((heads, local_rows), f32),
        ),
        in_specs=[hbm] * 6 + [vmem] * 2,
        out_specs=(vmem, vmem),
        scratch_shapes=[
            pltpu.VMEM(tokens.shape, bf16),
            pltpu.VMEM(w_query.shape, bf16),
            pltpu.VMEM(w_key.shape, bf16),
            pltpu.VMEM(w_value.shape, bf16),
            pltpu.VMEM((local_rows, width), bf16),
            pltpu.VMEM((local_rows, width), bf16),
            pltpu.VMEM((SEL, chosen.shape[0]), i32),
            pltpu.VMEM((chosen.shape[0], SEL), i32),
            pltpu.VMEM((local_rows, width), f32),
            pltpu.VMEM((local_rows, width), f32),
            pltpu.VMEM((4, nz, 128), i32),
            pltpu.SMEM((nz, 128), i32),
            pltpu.SMEM((8, 128), i32),
            pltpu.SMEM((nz, 128), i32),
            pltpu.SMEM((8, 128), i32),
            pltpu.VMEM((nz * blocks, BLK, 2 * width), bf16),
            pltpu.VMEM((nz * 8, BLK, 2 * width), bf16),
            pltpu.VMEM((ups * 8, BLK, 2 * width), bf16),
            pltpu.VMEM(stage, bf16),
            pltpu.VMEM(stage, bf16),
            pltpu.VMEM((SEL * BLK, 2 * width), bf16),
            pltpu.VMEM((ntp, width, w_out.shape[1]), bf16),
            pltpu.VMEM((local_rows, width), f32),
            pltpu.VMEM((local_rows, width), f32),
            pltpu.VMEM((local_rows, width), bf16),
            pltpu.VMEM((8, heads * BLK), f32),
            pltpu.VMEM((local_rows, width), bf16),
            pltpu.VMEM((8, heads * BLK), f32),
            pltpu.VMEM((local_rows, width), bf16),
            pltpu.VMEM((out_rows, ntp * width), bf16),
            dma((9,)),
            dma,
            dma((blocks * ups,)),
            dma((2 * (ups - 2),)),
            dma,
            dma((ups + 1,)),
            dma((2 * ups - 2,)),
            dma((2,)),
            dma,
            dma((4,)),
            dma((3,)),
            dma((3,)),
            dma,
            dma,
        ],
        compiler_params=pltpu.CompilerParams(
            collective_id=0, has_side_effects=True, vmem_limit_bytes=55000 * 1024
        ),
    )(tokens, w_query, w_key, w_value, w_out, chosen.T, cos_piece, sin_piece)
    return pl.pallas_call(
        finish,
        out_shape=(
            jax.ShapeDtypeStruct(mixed.shape, mixed.dtype),
            jax.ShapeDtypeStruct(log_sums.shape, log_sums.dtype),
        ),
        in_specs=[vmem, vmem],
        out_specs=(hbm, hbm),
        scratch_shapes=[dma((2,))],
        compiler_params=pltpu.CompilerParams(vmem_limit_bytes=1024 * 1024),
    )(mixed, log_sums)


def solution(mesh):
    placed = (P("kv", None), P(None, "tp"), P(None, "tp"), P(None, "tp"), P("tp", None), P())
    return jax.shard_map(
        functools.partial(local, mesh.shape["kv"], mesh.shape["tp"]),
        mesh=mesh,
        in_specs=placed,
        out_specs=(P(("kv", "tp"), None), P("tp", "kv")),
        check_vma=False,
    )
```

time: 64.8 us -> 57.2 us (0.88)
  the two profiles are of different devices: /device:TPU:487 before, /device:TPU:1 now
where the time goes in v4:
time: 57.2 us; the launch traced here: 57 us
  Pallas kernels  55.6 us (97%)
  between operations  0.67 us (1%)
    pallas_call x1, Pallas kernels, local(): pl.pallas_call(functools.partial(attend, nz, ntp), out_shape=(jax.ShapeDt...  54.9 us

profile of v4, /device:TPU:1, one launch (start us, length us, event | category | flops | bytes accessed | tf_op | source)
XLA Modules:
  0.0 57.0 jit_solution(2874028230006025602)
XLA Ops:
  0.7 0.0 copy-start
  0.7 0.2 multiply_sine_fusion
  0.8 0.6 copy-done
  1.4 54.9 %shard_map.77 = (bf16[32,2048]{1,0:T(8,128)(2,1)S(1)}, f32[2,256]{1,0:T(2,128)S(1)}) custom-call(bf16[256,2048]{1,0:T(8,128)(2,1)} %tokens_hbm.1, bf16[2048,128]{1,0:T(8,128)(2,1)} %wq_hbm.1, bf16[2048,128]{1,0:T(8,128)(2,1)} %wk_hbm.1, bf16[2048,128]{1,0:T(8,128)(2,1)} %wv_hbm.1, bf16[128,2048]{1,0:T(8,128)(2,1)} %w_hbm.1, s32[16,256]{1,0:T(8,128)S(1)} %bitcast.1, ...), custom_call_target="tpu_custom_call" | custom-call | tf_op jit(solution)/shard_map/pallas_call | solution.py:629
  56.3 0.7 %shard_map.78 = (bf16[32,2048]{1,0:T(8,128)(2,1)}, f32[2,256]{1,0:T(2,128)}) custom-call(bf16[32,2048]{1,0:T(8,128)(2,1)S(1)} %get-tuple-element.4.mixed_ref, f32[2,256]{1,0:T(2,128)S(1)} %get-tuple-element.5.log_ref), custom_call_target="tpu_custom_call" | custom-call | tf_op jit(solution)/shard_map/pallas_call | solution.py:687
  (2 shorter events, 0.0 us)
Async XLA Ops:
  0.7 0.7 %copy-start = (s32[256,16]{0,1:T(8,128)S(1)}, s32[256,16]{0,1:T(8,128)}, u32[]{:S(2)}) copy-start(s32[256,16]{0,1:T(8,128)} %param.11) | copy-start | bytes 49156

commit v5 on v4

--- a/solution.py
+++ b/solution.py
@@ -217,7 +217,6 @@
     ]
     for copy in to_smem:
         copy.start()
-    pl.semaphore_wait(barrier, 5 + ntp - 1)
 
     def remote(src, dst, send, recv, device):
         return pltpu.make_async_remote_copy(
@@ -229,15 +228,15 @@
             device_id_type=MESH,
         )
 
-    part = blocks // 2
-    parts = blocks // part
+    part = 1
+    parts = blocks
 
     def up_copy(step, b):
         at = pool.at[(z + nz - step) % nz * blocks + b]
         return remote(at, at, z_send, up_recv.at[step * blocks + b], (up, tp))
 
     def down_copy(step, b):
-        at = pool.at[pl.ds((z + step) % nz * blocks + b * part, part)]
+        at = pool.at[pl.ds((z + step) % nz * blocks + b, 1)]
         return remote(at, at, z_send, down_recv.at[step * parts + b], (down, tp))
 
     def stretch(size):
@@ -258,13 +257,22 @@
             self.sel = (sel_ref, far_sel_ref)[kind]
             self.recv = (y_recv, far_recv)[kind]
 
-        def right_copy(self, k, p):
-            dst = self.pool.at[pl.ds(3 * p, 3)]
-            return remote(to_right.at[self.stage + p], dst, y_send, self.recv.at[k], (right, tp))
-
-        def left_copy(self, k, p):
-            dst = self.pool.at[pl.ds(3 * self.planes + 3 * p, 3)]
-            return remote(to_left.at[self.stage + p], dst, y_send, self.recv.at[k], (left, tp))
+        def right_copy(self, p):
+            src, dst = to_right.at[self.stage + p, pl.ds(0, 2)], self.pool.at[pl.ds(3 * p, 2)]
+            return remote(src, dst, y_send, relay_recv.at[self.kind], (right, tp))
+
+        def left_copy(self, p):
+            src = to_left.at[self.stage + p, pl.ds(0, 2)]
+            dst = self.pool.at[pl.ds(3 * self.planes + 3 * p, 2)]
+            return remote(src, dst, y_send, relay_recv.at[self.kind], (left, tp))
+
+        def right_ahead(self, k, p):
+            src, dst = to_right.at[self.stage + p, 2], self.pool.at[3 * p + 2]
+            return remote(src, dst, y_send, self.recv.at[k], (right, tp))
+
+        def left_ahead(self, k, p):
+            src, dst = to_left.at[self.stage + p, 2], self.pool.at[3 * self.planes + 3 * p + 2]
+            return remote(src, dst, y_send, self.recv.at[k], (left, tp))
 
         def right_relay(self, p):
             src = self.pool.at[3 * p + 2]
@@ -287,17 +295,19 @@
                     found = jnp.where(which == b, here[b], found)
                 return found
 
+            to_right[at, 2] = pick(2, 0)
+            self.right_ahead(k, p).start()
+            to_left[at, 2] = pick(2, 1)
+            self.left_ahead(k, p).start()
             to_right[at, 0] = pick(1, 0)
             to_right[at, 1] = pick(1, 1)
-            to_right[at, 2] = pick(2, 0)
-            self.right_copy(k, p).start()
+            self.right_copy(p).start()
             to_left[at, 0] = pick(3, 0)
             to_left[at, 1] = pick(3, 1)
-            to_left[at, 2] = pick(2, 1)
-            self.left_copy(k, p).start()
+            self.left_copy(p).start()
 
         def relay(self, k, p):
-            arrived(6, self.recv.at[k])
+            arrived(2, self.recv.at[k])
             self.right_relay(p).start()
             self.left_relay(p).start()
 
@@ -352,6 +362,8 @@
     values = jnp.dot(tokens_ref[...], wv_ref[...], preferred_element_type=jnp.float32)
     values = values.astype(jnp.bfloat16)
     pool[pl.ds(z * blocks, blocks), :, width:] = values.reshape(blocks, BLK, width)
+
+    pl.semaphore_wait(barrier, 5 + ntp - 1)
 
     @pl.when(z < nz - 1)
     def _():
@@ -454,7 +466,7 @@
     def attention(i, queries, places, along, dest, low, high):
         for j in range(SEL):
             n = i * SEL + j
-            picked[j * BLK : (j + 1) * BLK, :] = jnp.where(
+            picked[i, j * BLK : (j + 1) * BLK, :] = jnp.where(
                 places[2, n] > 0, pool[places[0, n]], along[places[1, n]]
             )
         rows_here = queries[i * BLK : (i + 1) * BLK, :].astype(jnp.float32)
@@ -462,7 +474,7 @@
         stacked = jnp.where(wide_lane // HEAD_DIM == wide_row // BLK, stacked, 0.0)
         scores = lax.dot_general(
             stacked.astype(jnp.bfloat16),
-            picked[:, :width],
+            picked[i, :, :width],
             (((1,), (1,)), ((), ())),
             preferred_element_type=jnp.float32,
         )
@@ -475,7 +487,7 @@
         weights = jnp.exp(scores - top)
         total = jnp.sum(weights, axis=1, keepdims=True)
         summed = jnp.dot(
-            weights.astype(jnp.bfloat16), picked[:, width:], preferred_element_type=jnp.float32
+            weights.astype(jnp.bfloat16), picked[i, :, width:], preferred_element_type=jnp.float32
         )
         return by_head(summed / total), top + jnp.log(total)
 
@@ -483,7 +495,7 @@
 
     def own_attention():
         for c in range(nz):
-            pl.when(z == c)(lambda: arrived(2 * plane_counts(c)[0], relay_recv.at[0]))
+            pl.when(z == c)(lambda: arrived(6 * plane_counts(c)[0], relay_recv.at[0]))
         for i in range(blocks):
             result, column = attention(i, q_ref, idx_ref, own_pool, kv, first, nz * NY * blocks)
             mixed_ref[i * BLK : (i + 1) * BLK, :] = result
@@ -491,8 +503,50 @@
                 jnp.broadcast_to(column, (heads * BLK, width))
             )
 
+    def part_copy(to):
+        src = att.at[pl.ds(to * rows, rows)]
+        dst = abuf.at[:, pl.ds(pl.multiple_of(tp * width, width), width)]
+        return remote(src, dst, a_send, a_recv, (kv, to))
+
+    def emit():
+        per_block = ntp // blocks
+        for i in range(blocks):
+            at = slice(i * BLK, (i + 1) * BLK)
+            att[at, :] = mixed_ref[at, :].astype(jnp.bfloat16)
+            for to in range(i * per_block, (i + 1) * per_block):
+
+                @pl.when(to != tp)
+                def _():
+                    part_copy(to).start()
+
+                @pl.when(to == tp)
+                def _():
+                    abuf[:, pl.ds(pl.multiple_of(tp * width, width), width)] = att[
+                        to * rows : (to + 1) * rows, :
+                    ]
+
+        for head in range(heads):
+            cols = slice(head * HEAD_DIM, (head + 1) * HEAD_DIM)
+            lse_ref[head : head + 1, :] = jnp.concatenate(
+                [
+                    jnp.sum(
+                        jnp.where(
+                            eye[:BLK, :HEAD_DIM], wide_ref[i * BLK : (i + 1) * BLK, cols], 0.0
+                        ),
+                        axis=0,
+                        keepdims=True,
+                    )
+                    for i in range(blocks)
+                ],
+                axis=1,
+            )
+
     early = z <= 1
-    pl.when(early)(own_attention)
+
+    @pl.when(early)
+    def _():
+        own_attention()
+        emit()
 
     @pl.when(helper)
     def _():
@@ -500,7 +554,7 @@
 
             @pl.when(z == c)
             def _():
-                arrived(2 * plane_counts(c)[1], relay_recv.at[1])
+                arrived(6 * plane_counts(c)[1], relay_recv.at[1])
 
         q_copy.wait_recv()
         help_log_out[...] = jnp.zeros(help_log_out.shape, jnp.float32)
@@ -531,42 +585,7 @@
             mixed_ref[at, :] = (mixed_ref[at, :] * share + extra * other) / total
             wide_ref[at, :] = top + jnp.log(total)
 
-    def part_copy(to):
-        src = att.at[pl.ds(to * rows, rows)]
-        dst = abuf.at[:, pl.ds(pl.multiple_of(tp * width, width), width)]
-        return remote(src, dst, a_send, a_recv, (kv, to))
-
-    per_block = ntp // blocks
-    for i in range(blocks):
-        at = slice(i * BLK, (i + 1) * BLK)
-        att[at, :] = mixed_ref[at, :].astype(jnp.bfloat16)
-        for to in range(i * per_block, (i + 1) * per_block):
-
-            @pl.when(to != tp)
-            def _():
-                part_copy(to).start()
-
-            @pl.when(to == tp)
-            def _():
-                abuf[:, pl.ds(pl.multiple_of(tp * width, width), width)] = att[
-                    to * rows : (to + 1) * rows, :
-                ]
-
-    for head in range(heads):
-        cols = slice(head * HEAD_DIM, (head + 1) * HEAD_DIM)
-        lse_ref[head : head + 1, :] = jnp.concatenate(
-            [
-                jnp.sum(
-                    jnp.where(
-                        eye[:BLK, :HEAD_DIM], wide_ref[i * BLK : (i + 1) * BLK, cols], 0.0
-                    ),
-                    axis=0,
-                    keepdims=True,
-                )
-                for i in range(blocks)
-            ],
-            axis=1,
-        )
+    pl.when(z > 1)(emit)
 
     for c in range(nz):
 
@@ -655,7 +674,7 @@
             pltpu.VMEM((ups * 8, BLK, 2 * width), bf16),
             pltpu.VMEM(stage, bf16),
             pltpu.VMEM(stage, bf16),
-            pltpu.VMEM((SEL * BLK, 2 * width), bf16),
+            pltpu.VMEM((blocks, SEL * BLK, 2 * width), bf16),
             pltpu.VMEM((ntp, width, w_out.shape[1]), bf16),
             pltpu.VMEM((local_rows, width), f32),
             pltpu.VMEM((local_rows, width), f32),
@@ -668,7 +687,7 @@
             dma((9,)),
             dma,
             dma((blocks * ups,)),
-            dma((2 * (ups - 2),)),
+            dma((blocks * (ups - 2),)),
             dma,
             dma((ups + 1,)),
             dma((2 * ups - 2,)),

time: 57.2 us -> 51.9 us (0.907)
  Pallas kernels: 55.6 us -> 50 us
    pallas_call x1, Pallas kernels: 54.9 us -> 49.3 us  [local(): pl.pallas_call(functools.partial(attend, nz, ntp), out_shape=(jax.ShapeDt...]
where the time goes in v5:
time: 51.9 us; the launch traced here: 51.4 us
  Pallas kernels  50 us (96%)
  between operations  0.67 us (1%)
  local copies, waits for them, and re-layouts  0.56 us (1%)
    pallas_call x1, Pallas kernels, local(): pl.pallas_call(functools.partial(attend, nz, ntp), out_shape=(jax.ShapeDt...  49.3 us

profile of v5, /device:TPU:1, one launch (start us, length us, event | category | flops | bytes accessed | tf_op | source)
XLA Modules:
  0.0 51.4 jit_solution(9449936319512820402)
XLA Ops:
  0.7 0.0 copy-start
  0.7 0.2 multiply_sine_fusion
  0.8 0.6 %copy-done = s32[256,16]{0,1:T(8,128)S(1)} copy-done((s32[256,16]{0,1:T(8,128)S(1)}, s32[256,16]{0,1:T(8,128)}, u32[]{:S(2)}) %copy-start) | copy-done | bytes 16408
  1.4 49.3 %shard_map.77 = (bf16[32,2048]{1,0:T(8,128)(2,1)S(1)}, f32[2,256]{1,0:T(2,128)S(1)}) custom-call(bf16[256,2048]{1,0:T(8,128)(2,1)} %tokens_hbm.1, bf16[2048,128]{1,0:T(8,128)(2,1)} %wq_hbm.1, bf16[2048,128]{1,0:T(8,128)(2,1)} %wk_hbm.1, bf16[2048,128]{1,0:T(8,128)(2,1)} %wv_hbm.1, bf16[128,2048]{1,0:T(8,128)(2,1)} %w_hbm.1, s32[16,256]{1,0:T(8,128)S(1)} %bitcast.1, ...), custom_call_target="tpu_custom_call" | custom-call | tf_op jit(solution)/shard_map/pallas_call | solution.py:648
  50.7 0.7 %shard_map.78 = (bf16[32,2048]{1,0:T(8,128)(2,1)}, f32[2,256]{1,0:T(2,128)}) custom-call(bf16[32,2048]{1,0:T(8,128)(2,1)S(1)} %get-tuple-element.4.mixed_ref, f32[2,256]{1,0:T(2,128)S(1)} %get-tuple-element.5.log_ref), custom_call_target="tpu_custom_call" | custom-call | tf_op jit(solution)/shard_map/pallas_call | solution.py:706
  (2 shorter events, 0.0 us)
Async XLA Ops:
  0.7 0.7 %copy-start = (s32[256,16]{0,1:T(8,128)S(1)}, s32[256,16]{0,1:T(8,128)}, u32[]{:S(2)}) copy-start(s32[256,16]{0,1:T(8,128)} %param.11) | copy-start | bytes 49156

commit v6 on v5

--- a/solution.py
+++ b/solution.py
@@ -120,8 +120,7 @@
     lse_ref,
     tokens_ref,
     wq_ref,
-    wk_ref,
-    wv_ref,
+    wkv_ref,
     q_ref,
     q_far,
     chosen_across,
@@ -170,27 +169,29 @@
     x, core = tp // 2, tp % 2
     up = ((z + 1) % nz) * NY + y
     down = ((z + nz - 1) % nz) * NY + y
-    mirror_z = nz - 1 - z
+    outer, place_in = (z // 4 + 1) // 2 % 2, z % 4
+    mirror_z = (3 - z // 4) * 4
+    mirror_z += outer * (3 - place_in) + (1 - outer) * (place_in + 1 - 2 * (place_in % 2))
     mirror = mirror_z * NY + y
     right = z * NY + (y + 1) % NY
     left = z * NY + (y + NY - 1) % NY
     x_right = ((x + 1) % nx) * 2 + core
     x_left = ((x + nx - 1) % nx) * 2 + core
     partner = x * 2 + (1 - core)
-    width = wk_ref.shape[1]
+    width = wq_ref.shape[1]
     blocks = att.shape[0] // BLK
     heads = width // HEAD_DIM
     rows = att.shape[0] // ntp
     ups = nz // 2
-    last_far = ups - 2 - z
+    last_far = mirror_z - ups - 1
 
     def load(which, src, dst):
         return pltpu.make_async_copy(src, dst, local_sem.at[which])
 
     loads = [
         load(0, tokens_hbm, tokens_ref),
-        load(1, wk_hbm, wk_ref),
-        load(2, wv_hbm, wv_ref),
+        load(1, wk_hbm, wkv_ref.at[:, pl.ds(0, width)]),
+        load(2, wv_hbm, wkv_ref.at[:, pl.ds(width, width)]),
         load(3, w_hbm, wall.at[tp]),
         load(4, wq_hbm, wq_ref),
     ]
@@ -232,8 +233,8 @@
     parts = blocks
 
     def up_copy(step, b):
-        at = pool.at[(z + nz - step) % nz * blocks + b]
-        return remote(at, at, z_send, up_recv.at[step * blocks + b], (up, tp))
+        at = pool.at[(z + nz - step) % nz * blocks + b // 2, pl.ds(b % 2 * (BLK // 2), BLK // 2)]
+        return remote(at, at, z_send, up_recv.at[step * 2 * blocks + b], (up, tp))
 
     def down_copy(step, b):
         at = pool.at[pl.ds((z + step) % nz * blocks + b, 1)]
@@ -350,27 +351,28 @@
     o_copy = remote(help_out, help_in, help_send.at[1], help_recv.at[1], (mirror, tp))
     log_copy = remote(help_log_out, help_log_in, help_send.at[2], help_recv.at[2], (mirror, tp))
     helper = last_far >= 0
-    helped = mirror_z <= ups - 2
+    helped = z >= ups + 1
 
     loads[0].wait()
     loads[1].wait()
     cos_part, sin_part = cos_ref[...], sin_ref[...]
-    keys = jnp.dot(tokens_ref[...], wk_ref[...], preferred_element_type=jnp.float32)
-    keys = turn(keys, cos_part, sin_part).astype(jnp.bfloat16)
+    loads[2].wait()
+    both = jnp.dot(tokens_ref[...], wkv_ref[...], preferred_element_type=jnp.float32)
+    keys = turn(both[:, :width], cos_part, sin_part).astype(jnp.bfloat16)
     pool[pl.ds(z * blocks, blocks), :, :width] = keys.reshape(blocks, BLK, width)
-    loads[2].wait()
-    values = jnp.dot(tokens_ref[...], wv_ref[...], preferred_element_type=jnp.float32)
-    values = values.astype(jnp.bfloat16)
+    values = both[:, width:].astype(jnp.bfloat16)
     pool[pl.ds(z * blocks, blocks), :, width:] = values.reshape(blocks, BLK, width)
-
     pl.semaphore_wait(barrier, 5 + ntp - 1)
 
     @pl.when(z < nz - 1)
     def _():
-        for b in range(blocks):
+        for b in range(2 * blocks):
             up_copy(0, b).start()
 
-    goes_down = (z >= 1) & (z <= ups - 2)
+    def from_above(r, p):
+        return (p > r) & ((p <= 4) | ((r >= 2) & (p <= 6)))
+
+    goes_down = (z >= 1) & (z <= 6)
 
     @pl.when(goes_down)
     def _():
@@ -402,7 +404,7 @@
 
     def relay_step(k):
         pl.when(far_below(k))(lambda: routes[1].relay(k, z - k))
-        if 1 <= k <= ups - 2:
+        if 1 <= k <= 4:
             pl.when(far_above(k - 1))(lambda: routes[1].relay(ups + k - 1, z + k))
         pl.when(own_there(k))(lambda: routes[0].relay(k, z - k))
 
@@ -411,23 +413,23 @@
 
         @pl.when(own_there(k))
         def _():
-            for b in range(blocks):
-                remote(pool.at[b], pool.at[b], z_send, up_recv.at[step * blocks + b], (up, tp)).wait_recv()
+            for b in range(2 * blocks):
+                up_copy(step, b).wait_recv()
                 if step + 1 < ups:
                     pl.when(z < nz - 1)(lambda: up_copy(step + 1, b).start())
             pl.when(z - k <= last_far)(lambda: routes[1].exchange(k, z - k))
             routes[0].exchange(k, z - k)
 
-        if step <= ups - 3:
-
-            @pl.when(z + 1 + step <= ups - 2)
+        if step <= 3:
+
+            @pl.when((z <= 5) & from_above(z, z + 1 + step))
             def _():
                 for b in range(parts):
                     arrived(part, down_recv.at[step * parts + b])
 
-                    if step <= ups - 4:
-
-                        @pl.when(z >= 1)
+                    if step <= 2:
+
+                        @pl.when((z >= 1) & from_above(z - 1, z + 1 + step))
                         def _():
                             down_copy(step + 1, b).start()
 
@@ -437,16 +439,18 @@
             w_first()
         if step == 5:
             w_second()
-        if step >= 1:
-            relay_step(step - 1)
-    relay_step(ups - 1)
-    relay_step(ups)
+        if step >= 2:
+            relay_step(step - 2)
+    relay_step(6)
+    relay_step(7)
+    relay_step(8)
+
 
     def plane_counts(c):
         own = min(c, ups) + 1
-        far = max(0, ups - 1 - c)
+        far = (5, 4, 7, 6, 3, 2, 1)[c] if c <= 6 else 0
         ups_sent = min(c, ups - 1) + 1 if c < nz - 1 else 0
-        downs_sent = ups - 1 - c if 1 <= c <= ups - 2 else 0
+        downs_sent = (0, 4, 3, 4, 3, 2, 1)[c] if c <= 6 else 0
         return own, far, (ups_sent + downs_sent) * blocks
 
     lane = lax.broadcasted_iota(jnp.int32, (BLK, width), 1)
@@ -656,8 +660,7 @@
         scratch_shapes=[
             pltpu.VMEM(tokens.shape, bf16),
             pltpu.VMEM(w_query.shape, bf16),
-            pltpu.VMEM(w_key.shape, bf16),
-            pltpu.VMEM(w_value.shape, bf16),
+            pltpu.VMEM((w_key.shape[0], 2 * width), bf16),
             pltpu.VMEM((local_rows, width), bf16),
             pltpu.VMEM((local_rows, width), bf16),
             pltpu.VMEM((SEL, chosen.shape[0]), i32),
@@ -686,11 +689,11 @@
             pltpu.VMEM((out_rows, ntp * width), bf16),
             dma((9,)),
             dma,
-            dma((blocks * ups,)),
-            dma((blocks * (ups - 2),)),
+            dma((2 * blocks * ups,)),
+            dma((blocks * 4,)),
             dma,
             dma((ups + 1,)),
-            dma((2 * ups - 2,)),
+            dma((ups + 4,)),
             dma((2,)),
             dma,
             dma((4,)),

time: 51.9 us -> 55.3 us (1.066)
  the two profiles are of different devices: /device:TPU:1 before, /device:TPU:65 now
where the time goes in v6:
time: 55.3 us; the launch traced here: 55.1 us
  Pallas kernels  53.7 us (97%)
  between operations  0.67 us (1%)
  local copies, waits for them, and re-layouts  0.56 us (1%)
    pallas_call x1, Pallas kernels, local(): pl.pallas_call(functools.partial(attend, nz, ntp), out_shape=(jax.ShapeDt...  53 us

profile of v6, /device:TPU:65, one launch (start us, length us, event | category | flops | bytes accessed | tf_op | source)
XLA Modules:
  0.0 55.1 jit_solution(7217585628269489736)
XLA Ops:
  0.7 0.0 copy-start
  0.7 0.2 multiply_sine_fusion
  0.8 0.6 %copy-done = s32[256,16]{0,1:T(8,128)S(1)} copy-done((s32[256,16]{0,1:T(8,128)S(1)}, s32[256,16]{0,1:T(8,128)}, u32[]{:S(2)}) %copy-start) | copy-done | bytes 16408
  1.4 53.0 %shard_map.77 = (bf16[32,2048]{1,0:T(8,128)(2,1)S(1)}, f32[2,256]{1,0:T(2,128)S(1)}) custom-call(bf16[256,2048]{1,0:T(8,128)(2,1)} %tokens_hbm.1, bf16[2048,128]{1,0:T(8,128)(2,1)} %wq_hbm.1, bf16[2048,128]{1,0:T(8,128)(2,1)} %wk_hbm.1, bf16[2048,128]{1,0:T(8,128)(2,1)} %wv_hbm.1, bf16[128,2048]{1,0:T(8,128)(2,1)} %w_hbm.1, s32[16,256]{1,0:T(8,128)S(1)} %bitcast.1, ...), custom_call_target="tpu_custom_call" | custom-call | tf_op jit(solution)/shard_map/pallas_call | solution.py:652
  54.4 0.7 %shard_map.78 = (bf16[32,2048]{1,0:T(8,128)(2,1)}, f32[2,256]{1,0:T(2,128)}) custom-call(bf16[32,2048]{1,0:T(8,128)(2,1)S(1)} %get-tuple-element.4.mixed_ref, f32[2,256]{1,0:T(2,128)S(1)} %get-tuple-element.5.log_ref), custom_call_target="tpu_custom_call" | custom-call | tf_op jit(solution)/shard_map/pallas_call | solution.py:709
  (2 shorter events, 0.0 us)
Async XLA Ops:
  0.7 0.7 %copy-start = (s32[256,16]{0,1:T(8,128)S(1)}, s32[256,16]{0,1:T(8,128)}, u32[]{:S(2)}) copy-start(s32[256,16]{0,1:T(8,128)} %param.11) | copy-start | bytes 49156

commit v7 on v5

--- a/solution.py
+++ b/solution.py
@@ -120,8 +120,7 @@
     lse_ref,
     tokens_ref,
     wq_ref,
-    wk_ref,
-    wv_ref,
+    wkv_ref,
     q_ref,
     q_far,
     chosen_across,
@@ -177,7 +176,7 @@
     x_right = ((x + 1) % nx) * 2 + core
     x_left = ((x + nx - 1) % nx) * 2 + core
     partner = x * 2 + (1 - core)
-    width = wk_ref.shape[1]
+    width = wq_ref.shape[1]
     blocks = att.shape[0] // BLK
     heads = width // HEAD_DIM
     rows = att.shape[0] // ntp
@@ -189,8 +188,8 @@
 
     loads = [
         load(0, tokens_hbm, tokens_ref),
-        load(1, wk_hbm, wk_ref),
-        load(2, wv_hbm, wv_ref),
+        load(1, wk_hbm, wkv_ref.at[:, pl.ds(0, width)]),
+        load(2, wv_hbm, wkv_ref.at[:, pl.ds(width, width)]),
         load(3, w_hbm, wall.at[tp]),
         load(4, wq_hbm, wq_ref),
     ]
@@ -355,14 +354,12 @@
     loads[0].wait()
     loads[1].wait()
     cos_part, sin_part = cos_ref[...], sin_ref[...]
-    keys = jnp.dot(tokens_ref[...], wk_ref[...], preferred_element_type=jnp.float32)
-    keys = turn(keys, cos_part, sin_part).astype(jnp.bfloat16)
+    loads[2].wait()
+    both = jnp.dot(tokens_ref[...], wkv_ref[...], preferred_element_type=jnp.float32)
+    keys = turn(both[:, :width], cos_part, sin_part).astype(jnp.bfloat16)
     pool[pl.ds(z * blocks, blocks), :, :width] = keys.reshape(blocks, BLK, width)
-    loads[2].wait()
-    values = jnp.dot(tokens_ref[...], wv_ref[...], preferred_element_type=jnp.float32)
-    values = values.astype(jnp.bfloat16)
+    values = both[:, width:].astype(jnp.bfloat16)
     pool[pl.ds(z * blocks, blocks), :, width:] = values.reshape(blocks, BLK, width)
-
     pl.semaphore_wait(barrier, 5 + ntp - 1)
 
     @pl.when(z < nz - 1)
@@ -656,8 +653,7 @@
         scratch_shapes=[
             pltpu.VMEM(tokens.shape, bf16),
             pltpu.VMEM(w_query.shape, bf16),
-            pltpu.VMEM(w_key.shape, bf16),
-            pltpu.VMEM(w_value.shape, bf16),
+            pltpu.VMEM((w_key.shape[0], 2 * width), bf16),
             pltpu.VMEM((local_rows, width), bf16),
             pltpu.VMEM((local_rows, width), bf16),
             pltpu.VMEM((SEL, chosen.shape[0]), i32),

time: 51.9 us -> 51.9 us (level)
  no operation moved by 1% of the time
where the time goes in v7:
time: 51.9 us; the launch traced here: 51.4 us
  Pallas kernels  50 us (96%)
  between operations  0.67 us (1%)
  local copies, waits for them, and re-layouts  0.56 us (1%)
    pallas_call x1, Pallas kernels, local(): pl.pallas_call(functools.partial(attend, nz, ntp), out_shape=(jax.ShapeDt...  49.3 us

profile of v7, /device:TPU:1, one launch (start us, length us, event | category | flops | bytes accessed | tf_op | source)
XLA Modules:
  0.0 51.4 jit_solution(17035414334733477668)
XLA Ops:
  0.7 0.0 copy-start
  0.7 0.2 multiply_sine_fusion
  0.8 0.6 %copy-done = s32[256,16]{0,1:T(8,128)S(1)} copy-done((s32[256,16]{0,1:T(8,128)S(1)}, s32[256,16]{0,1:T(8,128)}, u32[]{:S(2)}) %copy-start) | copy-done | bytes 16408
  1.4 49.3 %shard_map.77 = (bf16[32,2048]{1,0:T(8,128)(2,1)S(1)}, f32[2,256]{1,0:T(2,128)S(1)}) custom-call(bf16[256,2048]{1,0:T(8,128)(2,1)} %tokens_hbm.1, bf16[2048,128]{1,0:T(8,128)(2,1)} %wq_hbm.1, bf16[2048,128]{1,0:T(8,128)(2,1)} %wk_hbm.1, bf16[2048,128]{1,0:T(8,128)(2,1)} %wv_hbm.1, bf16[128,2048]{1,0:T(8,128)(2,1)} %w_hbm.1, s32[16,256]{1,0:T(8,128)S(1)} %bitcast.1, ...), custom_call_target="tpu_custom_call" | custom-call | tf_op jit(solution)/shard_map/pallas_call | solution.py:645
  50.7 0.7 %shard_map.78 = (bf16[32,2048]{1,0:T(8,128)(2,1)}, f32[2,256]{1,0:T(2,128)}) custom-call(bf16[32,2048]{1,0:T(8,128)(2,1)S(1)} %get-tuple-element.4.mixed_ref, f32[2,256]{1,0:T(2,128)S(1)} %get-tuple-element.5.log_ref), custom_call_target="tpu_custom_call" | custom-call | tf_op jit(solution)/shard_map/pallas_call | solution.py:702
  (2 shorter events, 0.0 us)
Async XLA Ops:
  0.7 0.7 %copy-start = (s32[256,16]{0,1:T(8,128)S(1)}, s32[256,16]{0,1:T(8,128)}, u32[]{:S(2)}) copy-start(s32[256,16]{0,1:T(8,128)} %param.11) | copy-start | bytes 49156

commit v8 on v7

--- a/solution.py
+++ b/solution.py
@@ -147,6 +147,7 @@
     help_log_in,
     att,
     abuf,
+    acc_ref,
     local_sem,
     z_send,
     up_recv,
@@ -227,15 +228,14 @@
             device_id_type=MESH,
         )
 
-    part = 1
-    parts = blocks
+    parts = 2 * blocks
 
     def up_copy(step, b):
-        at = pool.at[(z + nz - step) % nz * blocks + b]
-        return remote(at, at, z_send, up_recv.at[step * blocks + b], (up, tp))
+        at = pool.at[(z + nz - step) % nz * blocks + b // 2, pl.ds(b % 2 * (BLK // 2), BLK // 2)]
+        return remote(at, at, z_send, up_recv.at[step * 2 * blocks + b], (up, tp))
 
     def down_copy(step, b):
-        at = pool.at[pl.ds((z + step) % nz * blocks + b, 1)]
+        at = pool.at[(z + step) % nz * blocks + b // 2, pl.ds(b % 2 * (BLK // 2), BLK // 2)]
         return remote(at, at, z_send, down_recv.at[step * parts + b], (down, tp))
 
     def stretch(size):
@@ -364,7 +364,7 @@
 
     @pl.when(z < nz - 1)
     def _():
-        for b in range(blocks):
+        for b in range(2 * blocks):
             up_copy(0, b).start()
 
     goes_down = (z >= 1) & (z <= ups - 2)
@@ -408,8 +408,8 @@
 
         @pl.when(own_there(k))
         def _():
-            for b in range(blocks):
-                remote(pool.at[b], pool.at[b], z_send, up_recv.at[step * blocks + b], (up, tp)).wait_recv()
+            for b in range(2 * blocks):
+                up_copy(step, b).wait_recv()
                 if step + 1 < ups:
                     pl.when(z < nz - 1)(lambda: up_copy(step + 1, b).start())
             pl.when(z - k <= last_far)(lambda: routes[1].exchange(k, z - k))
@@ -420,7 +420,7 @@
             @pl.when(z + 1 + step <= ups - 2)
             def _():
                 for b in range(parts):
-                    arrived(part, down_recv.at[step * parts + b])
+                    down_copy(step, b).wait_recv()
 
                     if step <= ups - 4:
 
@@ -500,10 +500,10 @@
                 jnp.broadcast_to(column, (heads * BLK, width))
             )
 
-    def part_copy(to):
+    def part_copy(to, distant):
         src = att.at[pl.ds(to * rows, rows)]
         dst = abuf.at[:, pl.ds(pl.multiple_of(tp * width, width), width)]
-        return remote(src, dst, a_send, a_recv, (kv, to))
+        return remote(src, dst, a_send, a_recv.at[distant], (kv, to))
 
     def emit():
         per_block = ntp // blocks
@@ -512,9 +512,15 @@
             att[at, :] = mixed_ref[at, :].astype(jnp.bfloat16)
             for to in range(i * per_block, (i + 1) * per_block):
 
-                @pl.when(to != tp)
+                opposite = (to // 2 - x + nx) % nx == nx // 2
+
+                @pl.when((to != tp) & opposite)
                 def _():
-                    part_copy(to).start()
+                    part_copy(to, 1).start()
+
+                @pl.when((to != tp) & jnp.logical_not(opposite))
+                def _():
+                    part_copy(to, 0).start()
 
                 @pl.when(to == tp)
                 def _():
@@ -602,20 +608,27 @@
     w_arrived(4, w_recv.at[3])
     sent_w = wall.at[pl.ds(0, ntp - 1)]
     remote(sent_w, sent_w, w_send, w_recv.at[3], (kv, partner)).wait_send()
-    others = abuf.at[:, pl.ds(0, (ntp - 1) * width)]
-    remote(others, others, a_send, a_recv, (kv, partner)).wait()
+    def parts_of(count):
+        return abuf.at[:, pl.ds(0, count * width)]
+
     total_width = out_ref.shape[1]
     chunk = min(512, total_width)
+
+    def product(chip, cols):
+        lhs = abuf[:, pl.ds(pl.multiple_of(chip * 2 * width, 2 * width), 2 * width)]
+        rhs = wall[pl.ds(2 * chip, 2), :, cols].reshape(2 * width, chunk)
+        return jnp.dot(lhs, rhs, preferred_element_type=jnp.float32)
+
+    remote(parts_of(ntp - 3), parts_of(ntp - 3), a_send, a_recv.at[0], (kv, partner)).wait_recv()
     for c in range(total_width // chunk):
         cols = slice(c * chunk, (c + 1) * chunk)
-        acc = jnp.zeros((rows, chunk), jnp.float32)
-        for t in range(ntp):
-            acc += jnp.dot(
-                abuf[:, t * width : (t + 1) * width],
-                wall[t, :, cols],
-                preferred_element_type=jnp.float32,
-            )
-        out_ref[:, cols] = acc.astype(jnp.bfloat16)
+        near_sum = product(x, cols) + product((x + 1) % nx, cols) + product((x + 3) % nx, cols)
+        acc_ref[:, cols] = near_sum
+    remote(parts_of(2), parts_of(2), a_send, a_recv.at[1], (kv, partner)).wait_recv()
+    for c in range(total_width // chunk):
+        cols = slice(c * chunk, (c + 1) * chunk)
+        out_ref[:, cols] = (acc_ref[:, cols] + product((x + 2) % nx, cols)).astype(jnp.bfloat16)
+    remote(parts_of(ntp - 1), parts_of(ntp - 1), a_send, a_recv.at[0], (kv, partner)).wait_send()
 
 
 def finish(mixed_ref, log_ref, mixed_out, log_out, sem):
@@ -680,10 +693,11 @@
             pltpu.VMEM((8, heads * BLK), f32),
             pltpu.VMEM((local_rows, width), bf16),
             pltpu.VMEM((out_rows, ntp * width), bf16),
+            pltpu.VMEM((out_rows, w_out.shape[1]), f32),
             dma((9,)),
             dma,
-            dma((blocks * ups,)),
-            dma((blocks * (ups - 2),)),
+            dma((2 * blocks * ups,)),
+            dma((2 * blocks * (ups - 2),)),
             dma,
             dma((ups + 1,)),
             dma((2 * ups - 2,)),
@@ -693,7 +707,7 @@
             dma((3,)),
             dma((3,)),
             dma,
-            dma,
+            dma((2,)),
         ],
         compiler_params=pltpu.CompilerParams(
             collective_id=0, has_side_effects=True, vmem_limit_bytes=55000 * 1024

time: 51.9 us -> 51.9 us (level)
  no operation moved by 1% of the time
where the time goes in v8:
time: 51.9 us; the launch traced here: 51.4 us
  Pallas kernels  50 us (96%)
  between operations  0.67 us (1%)
  local copies, waits for them, and re-layouts  0.56 us (1%)
    pallas_call x1, Pallas kernels, local(): pl.pallas_call(functools.partial(attend, nz, ntp), out_shape=(jax.ShapeDt...  49.3 us

profile of v8, /device:TPU:1, one launch (start us, length us, event | category | flops | bytes accessed | tf_op | source)
XLA Modules:
  0.0 51.4 jit_solution(2931798088332460893)
XLA Ops:
  0.7 0.0 copy-start
  0.7 0.2 multiply_sine_fusion
  0.8 0.6 %copy-done = s32[256,16]{0,1:T(8,128)S(1)} copy-done((s32[256,16]{0,1:T(8,128)S(1)}, s32[256,16]{0,1:T(8,128)}, u32[]{:S(2)}) %copy-start) | copy-done | bytes 16408
  1.4 49.3 %shard_map.77 = (bf16[32,2048]{1,0:T(8,128)(2,1)S(1)}, f32[2,256]{1,0:T(2,128)S(1)}) custom-call(bf16[256,2048]{1,0:T(8,128)(2,1)} %tokens_hbm.1, bf16[2048,128]{1,0:T(8,128)(2,1)} %wq_hbm.1, bf16[2048,128]{1,0:T(8,128)(2,1)} %wk_hbm.1, bf16[2048,128]{1,0:T(8,128)(2,1)} %wv_hbm.1, bf16[128,2048]{1,0:T(8,128)(2,1)} %w_hbm.1, s32[16,256]{1,0:T(8,128)S(1)} %bitcast.1, ...), custom_call_target="tpu_custom_call" | custom-call | tf_op jit(solution)/shard_map/pallas_call | solution.py:658
  50.7 0.7 %shard_map.78 = (bf16[32,2048]{1,0:T(8,128)(2,1)}, f32[2,256]{1,0:T(2,128)}) custom-call(bf16[32,2048]{1,0:T(8,128)(2,1)S(1)} %get-tuple-element.4.mixed_ref, f32[2,256]{1,0:T(2,128)S(1)} %get-tuple-element.5.log_ref), custom_call_target="tpu_custom_call" | custom-call | tf_op jit(solution)/shard_map/pallas_call | solution.py:716
  (2 shorter events, 0.0 us)
Async XLA Ops:
  0.7 0.7 %copy-start = (s32[256,16]{0,1:T(8,128)S(1)}, s32[256,16]{0,1:T(8,128)}, u32[]{:S(2)}) copy-start(s32[256,16]{0,1:T(8,128)} %param.11) | copy-start | bytes 49156
